TPU v7x, 256 devices: a 4x2x16 block of a 4x16x16 slice. The times are simulated.
256 devices in a mesh: grp: 2 (over y), sp: 32 (over z, core), tp: 4 (over x).
Axes of the slice: x: 4, y: 2, z: 16, core: 2. Of those that a mesh axis runs over, the one named last changes fastest.
The devices are a block of a 4x16x16 slice.
Arguments:
- queries: bfloat16 [32768, 2048], P(('grp', 'sp'), 'tp'), parts along dimension 0, may hold values from -64 to 64
- key_heads: bfloat16 [32768, 4, 64], P(('grp', 'sp'), 'tp'), parts along dimension 0, may hold values from -64 to 64
- value_heads: bfloat16 [32768, 4, 64], P(('grp', 'sp'), 'tp'), parts along dimension 0, may hold values from -6 to 6
- sink_logit: float32 [32], P('tp'), may hold values from 3 to 6
- out_weight: bfloat16 [2048, 2048], P('tp'), may hold values from -0.75 to 0.75
- residual: bfloat16 [32768, 2048], P(('grp', 'sp', 'tp')), parts along dimension 0, may hold values from -6 to 6
- norm_gain: float32 [2048], replicated, may hold values from 0.1 to 1.9
- expert_ids: int32 [32768, 2], P(('grp', 'sp', 'tp')), parts along dimension 0, may hold values from 0 to 127, all different within a row; in each aligned block of 128 rows (0 to 127, 128 to 255, ...) at most 4 rows name the same one
- route_weights: float32 [32768, 2], P(('grp', 'sp', 'tp')), parts along dimension 0, may hold values from 0.1 to 1
- gate_weight: bfloat16 [128, 2048, 512], P(('sp', 'tp')), may hold values from -0.125 to 0.125
- up_weight: bfloat16 [128, 2048, 512], P(('sp', 'tp')), may hold values from -0.125 to 0.125
- down_weight: bfloat16 [128, 512, 2048], P(('sp', 'tp')), may hold values from -0.5 to 0.5
Outputs:
- mixed: bfloat16 [32768, 2048], P(('grp', 'sp', 'tp')), parts along dimension 0
There are 2 independent parts, one for each index of `grp`. A program takes and returns all parts, laid end to end along the dimension named above; an argument that names none is the same for every part. Nothing has to cross between parts.
Inputs may be any that keep to these rules, and one draw needn't show every extreme that they name: `expert_ids`: each row names 2 different experts. In the rows of one device (aligned blocks of 128 rows) no expert is named more than 4 times, and in some blocks one expert is named exactly 4 times.
All inputs are finite; a program needn't handle non-finite values.
Results may differ from a plain program's by a relative error of at most 0.014.
Values may be sent and summed in bfloat16 or wider, within the bound.
A program may use at most 64 MiB of HBM per device.

v0:
```python
import jax
import jax.numpy as jnp
from jax import lax
from jax.sharding import PartitionSpec as P

WINDOW = 128


EPS = 1e-06


def from_behind(value, axis, steps):
    count = lax.axis_size(axis)
    initial, last = (max(0, -steps), min(count, count - steps))
    return lax.ppermute(value, axis, [(source, source + steps) for source in range(initial, last)])


def in_blocks(array, dim, devices):
    before, after = (array.shape[:dim], array.shape[dim + 1 :])
    return jnp.moveaxis(array.reshape(*before, devices, -1, *after), dim, 0)


def summed_on_arrival(array, axis, dim):
    blocks = in_blocks(array, dim, lax.axis_size(axis))
    arrived = lax.all_to_all(blocks, axis, split_axis=0, concat_axis=0, tiled=True)
    return arrived.sum(axis=0)


def on_device(
    queries,
    key_heads,
    value_heads,
    sink_logit,
    out_weight,
    residual,
    norm_gain,
    expert_ids,
    route_weights,
    gate_weight,
    up_weight,
    down_weight,
):
    rows_sp = queries.shape[0]
    kv_local = key_heads.shape[1]
    head_dim = key_heads.shape[2]
    heads_local = queries.shape[1] // head_dim
    group_size = heads_local // kv_local
    window = WINDOW
    count_of_blocks = rows_sp // window
    edge = jnp.stack([key_heads[rows_sp - window :], value_heads[rows_sp - window :]])
    tail_rows = from_behind(edge, "sp", 1)
    key_blocks = jnp.concatenate([tail_rows[0], key_heads], 0).reshape(
        count_of_blocks + 1, window, kv_local, head_dim
    )
    value_blocks = jnp.concatenate([tail_rows[1], value_heads], 0).reshape(
        count_of_blocks + 1, window, kv_local, head_dim
    )
    key_span = jnp.concatenate([key_blocks[:-1], key_blocks[1:]], 1)
    value_span = jnp.concatenate([value_blocks[:-1], value_blocks[1:]], 1)
    query_pos = jnp.arange(window, dtype=jnp.int32)[:, None]
    key_pos = jnp.arange(2 * window, dtype=jnp.int32)[None, :]
    distance = query_pos + window - key_pos
    band = (distance >= 0) & (distance < window)
    key_start = (
        lax.axis_index("sp") * rows_sp
        + jnp.arange(count_of_blocks, dtype=jnp.int32)[:, None] * window
        - window
        + key_pos
    )
    allowed = band[None, :, :] & (key_start >= 0)[:, None, :]
    query_blocks = queries.reshape(count_of_blocks, window, kv_local, group_size, head_dim)
    logit_scores = jnp.einsum(
        "bqhgd,bkhd->bhgqk", query_blocks, key_span, preferred_element_type=jnp.float32
    ) * head_dim ** (-0.5)
    logit_scores = jnp.where(allowed[:, None, None], logit_scores, -jnp.inf)
    sink_col = sink_logit.reshape(kv_local, group_size)[None, :, :, None, None]
    row_max = jnp.maximum(jnp.max(logit_scores, axis=-1, keepdims=True), sink_col)
    expd = jnp.exp(logit_scores - row_max)
    row_total = jnp.sum(expd, axis=-1, keepdims=True) + jnp.exp(sink_col - row_max)
    attention_probabilities = (expd / row_total).astype(jnp.bfloat16)
    attended = jnp.einsum(
        "bhgqk,bkhd->bqhgd", attention_probabilities, value_span, preferred_element_type=jnp.float32
    ).astype(jnp.bfloat16)
    attended = attended.reshape(rows_sp, heads_local * head_dim)
    rows_dev = residual.shape[0]
    width = residual.shape[1]
    projected = summed_on_arrival(
        jnp.dot(attended, out_weight, preferred_element_type=jnp.float32), "tp", 0
    )
    stream = (residual.astype(jnp.float32) + projected).astype(jnp.bfloat16)
    wide = stream.astype(jnp.float32)
    normed = (
        wide * lax.rsqrt(jnp.mean(wide * wide, axis=-1, keepdims=True) + EPS) * norm_gain
    ).astype(jnp.bfloat16)
    sp_count = lax.axis_size("sp")
    tp_count = lax.axis_size("tp")
    experts_total = sp_count * tp_count
    top_k = expert_ids.shape[1]
    capacity = max(2, 2 * top_k * rows_dev // experts_total)
    flat_ids = expert_ids.reshape(-1)
    pairs = flat_ids.shape[0]
    onehot = (flat_ids[:, None] == jnp.arange(experts_total, dtype=jnp.int32)[None, :]).astype(
        jnp.int32
    )
    earlier = jnp.cumsum(onehot, axis=0) - onehot
    slot_rank = jnp.sum(earlier * onehot, axis=1)
    flat_slot = flat_ids * capacity + slot_rank
    owner_row = jnp.arange(pairs, dtype=jnp.int32) // top_k
    token_in_slot = jnp.zeros((experts_total * capacity,), jnp.int32).at[flat_slot].set(owner_row)
    filled = jnp.zeros((experts_total * capacity,), jnp.bool_).at[flat_slot].set(True)
    outbox = jnp.where(filled[:, None], normed[token_in_slot], jnp.zeros((), jnp.bfloat16))
    outbox = outbox.reshape(experts_total, capacity, width)
    w_gate_own = gate_weight[0]
    w_up_own = up_weight[0]
    w_down_own = down_weight[0]
    arrived = lax.all_to_all(outbox, ("sp", "tp"), split_axis=0, concat_axis=0, tiled=True)
    rows = arrived.reshape(-1, width)
    gate = jnp.dot(rows, w_gate_own, preferred_element_type=jnp.float32)
    upward = jnp.dot(rows, w_up_own, preferred_element_type=jnp.float32)
    expert_hidden = (jax.nn.silu(gate) * upward).astype(jnp.bfloat16)
    expert_rows = jnp.dot(expert_hidden, w_down_own, preferred_element_type=jnp.float32).astype(
        jnp.bfloat16
    )
    results = expert_rows.reshape(arrived.shape)
    returned = lax.all_to_all(results, ("sp", "tp"), split_axis=0, concat_axis=0, tiled=True)
    picked_rows = returned.reshape(experts_total * capacity, width)[flat_slot].reshape(
        rows_dev, top_k, width
    )
    shares = route_weights / jnp.sum(route_weights, axis=-1, keepdims=True)
    combined = jnp.sum(shares[:, :, None] * picked_rows.astype(jnp.float32), axis=1)
    return (wide + combined).astype(jnp.bfloat16)


def solution(mesh):
    return jax.shard_map(
        on_device,
        mesh=mesh,
        in_specs=(
            P(("grp", "sp"), "tp"),
            P(("grp", "sp"), "tp", None),
            P(("grp", "sp"), "tp", None),
            P("tp"),
            P("tp", None),
            P(("grp", "sp", "tp"), None),
            P(),
            P(("grp", "sp", "tp"), None),
            P(("grp", "sp", "tp"), None),
            P(("sp", "tp"), None, None),
            P(("sp", "tp"), None, None),
            P(("sp", "tp"), None, None),
        ),
        out_specs=P(("grp", "sp", "tp"), None),
        check_vma=False,
    )
```

profile of v0, /device:TPU:33, one launch (start us, length us, event | category | flops | bytes accessed | tf_op | source)
XLA Modules:
  0.0 355.5 jit_solution(17730218004439928943)
XLA Ops:
  0.0 0.0 copy-start
  0.0 0.0 copy-start.2
  0.0 0.9 slice_bitcast_fusion.2
  0.9 5.7 %collective-permute-start = (bf16[2,128,1,64]{1,3,2,0:T(8,128)(2,1)S(1)}, bf16[2,128,1,64]{1,3,2,0:T(8,128)(2,1)S(1)}, u32[]{:S(2)}, u32[]{:S(2)}) collective-permute-start(bf16[2,128,1,64]{1,3,2,0:T(8,128)(2,1)S(1)} %pad_maximum_fusion.2), channel_id=1, source_target_pairs={{0,4},{4,8},{8,12},{12,16},{16,20},{20,24},{24,28},{28,32},{32,36}... | collective-permute-start | bytes 98312 | tf_op jit(solution)/shard_map/ppermute | solution.py:15
  6.7 0.9 copy_bitcast_fusion
  7.6 0.1 add_compare_fusion
  7.7 0.2 broadcast_and_fusion
  7.9 0.9 copy_bitcast_fusion.2
  8.7 1.6 reshape.236
  10.4 12.9 %collective-permute-done = bf16[2,128,1,64]{1,3,2,0:T(8,128)(2,1)S(1)} collective-permute-done((bf16[2,128,1,64]{1,3,2,0:T(8,128)(2,1)S(1)}, bf16[2,128,1,64]{1,3,2,0:T(8,128)(2,1)S(1)}, u32[]{:S(2)}, u32[]{:S(2)}) %collective-permute-start) | collective-permute-done | bytes 32800 | tf_op jit(solution)/shard_map/ppermute | solution.py:15
  23.3 0.0 copy-done.2
  23.3 0.0 copy-start.7
  23.3 0.9 fusion.1
  24.2 0.0 copy-done.7
  24.2 0.1 broadcast_maximum_fusion
  24.3 0.0 copy-start.3
  24.3 0.9 fusion
  25.2 0.1 exponential_add_fusion
  25.3 0.0 copy-done.3
  25.3 1.2 fusion.18
  26.5 0.0 copy-done
  26.6 3.3 fusion.7
  29.8 0.0 copy-start.5
  29.8 5.1 %all-to-all-start = ((f32[4,128,2048]{2,1,0:T(8,128)}), f32[4,128,2048]{2,1,0:T(8,128)}, u32[]{:S(2)}, u32[]{:S(2)}) async-start(f32[4,128,2048]{2,1,0:T(8,128)} %fusion.7), calls=%async_computation | async-start | bytes 8388608 | tf_op jit(solution)/shard_map/all_to_all | solution.py:25
  34.9 0.0 copy-done.5
  34.9 0.1 copy.27
  35.0 0.1 eq.29
  35.2 0.1 eq.25
  35.3 0.1 copy.29
  35.4 0.2 fusion.30
  35.7 0.1 copy.26
  35.8 0.1 mul.85
  36.0 0.2 fusion.36
  36.2 1.4 scatter_custom_fusion.1
  37.6 1.5 scatter_custom_fusion
  39.1 0.1 broadcast_in_dim.56
  39.3 0.0 copy-start.1
  39.3 41.4 %all-to-all-done = f32[4,128,2048]{2,1,0:T(8,128)} async-done(((f32[4,128,2048]{2,1,0:T(8,128)}), f32[4,128,2048]{2,1,0:T(8,128)}, u32[]{:S(2)}, u32[]{:S(2)}) %all-to-all-start) | async-done | bytes 4194336 | tf_op jit(solution)/shard_map/all_to_all | solution.py:25
  80.7 3.6 %reduce_sum.57 = f32[128,2048]{1,0:T(8,128)} reduce(f32[4,128,2048]{2,1,0:T(8,128)} %all-to-all-done, f32[]{:T(128)} %constant.29.clone.1), dimensions={0}, to_apply=%region_2.3 | reduce | flops 786432 | bytes 5242884 | tf_op jit(solution)/shard_map/reduce_sum | solution.py:26
  84.3 0.0 copy-done.1
  84.3 0.0 copy-start.4
  84.3 1.5 fusion.21
  85.8 0.0 copy-done.4
  85.8 0.2 fusion.23
  86.0 3.3 gather_fusion
  89.3 4.1 %gather.9 = bf16[128,4,2048]{2,1,0:T(4,128)(2,1)} reshape(bf16[512,2048]{1,0:T(8,128)(2,1)} %gather_fusion) | data formatting | bytes 4194304 | tf_op jit(solution)/shard_map/gather | solution.py:111
  93.4 2.6 broadcast_select_fusion
  96.0 113.8 %all_to_all.15 = bf16[128,4,2048]{2,1,0:T(4,128)(2,1)} all-to-all(bf16[128,4,2048]{2,1,0:T(4,128)(2,1)S(1)} %broadcast_select_fusion), channel_id=1, replica_groups=mesh['grp'=2,'sp'=32,'tp'=4] {'sp','tp'}, dimensions={0} | all-to-all | bytes 4194304 | tf_op jit(solution)/shard_map/all_to_all | solution.py:116
  209.8 4.0 %reshape.196 = bf16[512,2048]{1,0:T(8,128)(2,1)} reshape(bf16[128,4,2048]{2,1,0:T(4,128)(2,1)} %all_to_all.15) | data formatting | bytes 4194304 | tf_op jit(solution)/shard_map/reshape | solution.py:117
  213.8 4.4 %fusion.5 = f32[512,512]{1,0:T(8,128)} fusion(bf16[512,2048]{1,0:T(8,128)(2,1)} %reshape.196, bf16[1,2048,512]{2,1,0:T(8,128)(2,1)} %param.21), kind=kOutput, calls=%fused_computation.13 | convolution fusion | flops 1073741824 | bytes 5242880 | tf_op jit(solution)/shard_map/dot_general | solution.py:118
  218.2 6.9 %convolution_convert_fusion = bf16[512,2048]{1,0:T(8,128)(2,1)} fusion(bf16[1,512,2048]{2,1,0:T(8,128)(2,1)} %param.23, bf16[512,2048]{1,0:T(8,128)(2,1)} %reshape.196, bf16[1,2048,512]{2,1,0:T(8,128)(2,1)} %param.22, f32[512,512]{1,0:T(8,128)} %fusion.5), kind=kOutput, calls=%fused_computation.9 | convolution fusion | flops 2150105088 | bytes 9437184 | tf_op jit(solution)/shard_map/dot_general | solution.py:121
  225.1 4.1 %reshape.197 = bf16[128,4,2048]{2,1,0:T(4,128)(2,1)} reshape(bf16[512,2048]{1,0:T(8,128)(2,1)} %convolution_convert_fusion) | data formatting | bytes 4194304 | tf_op jit(solution)/shard_map/reshape | solution.py:124
  229.3 0.0 copy-start.6
  229.3 10.0 %all-to-all-start.2 = ((bf16[128,4,2048]{2,1,0:T(4,128)(2,1)}), bf16[128,4,2048]{2,1,0:T(4,128)(2,1)}, u32[]{:S(2)}, u32[]{:S(2)}) async-start(bf16[128,4,2048]{2,1,0:T(4,128)(2,1)} %reshape.197), calls=%async_computation.2 | async-start | bytes 4194304 | tf_op jit(solution)/shard_map/all_to_all | solution.py:125
  239.3 0.0 copy-done.6
  239.3 0.1 copy.25
  239.5 97.7 %all-to-all-done.2 = bf16[128,4,2048]{2,1,0:T(4,128)(2,1)} async-done(((bf16[128,4,2048]{2,1,0:T(4,128)(2,1)}), bf16[128,4,2048]{2,1,0:T(4,128)(2,1)}, u32[]{:S(2)}, u32[]{:S(2)}) %all-to-all-start.2) | async-done | bytes 2097184 | tf_op jit(solution)/shard_map/all_to_all | solution.py:125
  337.2 4.0 %reshape.198 = bf16[512,2048]{1,0:T(8,128)(2,1)} reshape(bf16[128,4,2048]{2,1,0:T(4,128)(2,1)} %all-to-all-done.2) | data formatting | bytes 4194304 | tf_op jit(solution)/shard_map/reshape | solution.py:126
  341.2 5.2 %gather_fusion.1 = bf16[256,2048]{1,0:T(8,128)(2,1)} fusion(bf16[512,2048]{1,0:T(8,128)(2,1)} %reshape.198, s32[1024]{0:T(1024)S(1)} %pad_clamp_fusion), kind=kCustom, calls=%fused_computation.1 | custom fusion | bytes 2098176 | tf_op jit(solution)/shard_map/gather | solution.py:126
  346.4 3.4 reshape.199
  349.8 4.8 %multiply_reduce_fusion = f32[128,2048]{1,0:T(8,128)S(1)} fusion(f32[128,2,2048]{2,1,0:T(2,128)} %reshape.199, f32[128,2]{1,0:T(8,128)S(1)} %copy.25), kind=kLoop, calls=%fused_computation.19 | loop fusion | flops 786432 | bytes 3146752 | tf_op jit(solution)/shard_map/reduce_sum | solution.py:130
  354.6 0.9 fusion.24
  (23 shorter events, 0.2 us)
Async XLA Ops:
  0.0 26.5 %copy-start = (bf16[512,2048]{1,0:T(8,128)(2,1)S(1)}, bf16[512,2048]{1,0:T(8,128)(2,1)}, u32[]{:S(2)}) copy-start(bf16[512,2048]{1,0:T(8,128)(2,1)} %param.16) | copy-start | bytes 6291460
  0.0 23.3 %copy-start.2 = (bf16[512,1,64]{0,2,1:T(8,128)(2,1)S(1)}, bf16[512,1,64]{0,2,1:T(8,128)(2,1)}, u32[]{:S(2)}) copy-start(bf16[512,1,64]{0,2,1:T(8,128)(2,1)} %param.13) | copy-start | bytes 196612
  0.9 22.4 %collective-permute-start = (bf16[2,128,1,64]{1,3,2,0:T(8,128)(2,1)S(1)}, bf16[2,128,1,64]{1,3,2,0:T(8,128)(2,1)S(1)}, u32[]{:S(2)}, u32[]{:S(2)}) collective-permute-start(bf16[2,128,1,64]{1,3,2,0:T(8,128)(2,1)S(1)} %pad_maximum_fusion.2), channel_id=1, source_target_pairs={{0,4},{4,8},{8,12},{12,16},{16,20},{20,24},{24,28},{28,32},{32,36}... | collective-permute-start | bytes 98312 | tf_op jit(solution)/shard_map/ppermute | solution.py:15
  23.3 0.9 copy-start.7
  24.3 1.0 copy-start.3
  29.8 5.1 %copy-start.5 = (s32[128,2]{0,1:T(2,128)S(1)}, s32[128,2]{0,1:T(2,128)}, u32[]{:S(2)}) copy-start(s32[128,2]{0,1:T(2,128)} %param.19) | copy-start | bytes 3076
  29.8 50.9 %all-to-all-start = ((f32[4,128,2048]{2,1,0:T(8,128)}), f32[4,128,2048]{2,1,0:T(8,128)}, u32[]{:S(2)}, u32[]{:S(2)}) async-start(f32[4,128,2048]{2,1,0:T(8,128)} %fusion.7), calls=%async_computation | async-start | bytes 8388608 | tf_op jit(solution)/shard_map/all_to_all | solution.py:25
  39.3 45.0 %copy-start.1 = (bf16[128,2048]{1,0:T(8,128)(2,1)S(1)}, bf16[128,2048]{1,0:T(8,128)(2,1)}, u32[]{:S(2)}) copy-start(bf16[128,2048]{1,0:T(8,128)(2,1)} %param.17) | copy-start | bytes 1572868
  84.3 1.5 copy-start.4
  229.3 10.0 %copy-start.6 = (f32[128,2]{0,1:T(2,128)S(1)}, f32[128,2]{0,1:T(2,128)}, u32[]{:S(2)}) copy-start(f32[128,2]{0,1:T(2,128)} %param.20) | copy-start | bytes 3076
  229.3 107.9 %all-to-all-start.2 = ((bf16[128,4,2048]{2,1,0:T(4,128)(2,1)}), bf16[128,4,2048]{2,1,0:T(4,128)(2,1)}, u32[]{:S(2)}, u32[]{:S(2)}) async-start(bf16[128,4,2048]{2,1,0:T(4,128)(2,1)} %reshape.197), calls=%async_computation.2 | async-start | bytes 4194304 | tf_op jit(solution)/shard_map/all_to_all | solution.py:125
where the time goes:
time: 356 us
  waiting for transfers between devices  152 us (43%)
  blocking collectives  114 us (32%)
  local copies, waits for them, and re-layouts  36.3 us (10%)
  starting transfers between devices  20.8 us (6%)
  matrix products  16.7 us (5%)
  other arithmetic  15.5 us (4%)
    all_to_all x1, blocking collectives, on_device(): lax.all_to_all(outbox, ('sp', 'tp'), split_axis=0, concat_axis=0, tiled=T...  114 us
    all_to_all x1, waiting for transfers between devices, on_device(): lax.all_to_all(results, ('sp', 'tp'), split_axis=0, concat_axis=0, tiled=...  97.7 us
    all_to_all x1, waiting for transfers between devices, summed_on_arrival(): lax.all_to_all(blocks, axis, split_axis=0, concat_axis=0, tiled=True)  41.4 us
    ppermute x1, waiting for transfers between devices, from_behind(): lax.ppermute(value, axis, [(source, source + steps) for source in range(i...  12.9 us
    all_to_all x1, starting transfers between devices, on_device(): lax.all_to_all(results, ('sp', 'tp'), split_axis=0, concat_axis=0, tiled=...  10 us
    gather x2, local copies, waits for them, and re-layouts, on_device(): normed[token_in_slot]  7.47 us
  transfers between devices with their start and end apart: 3, of which 3 were waited for; matrix products, arithmetic and copies ran while one was open for 2% of the time, Pallas kernels for 0%

commit v1 on v0

v1 whole, which is shorter than its diff:
```python
import functools

import jax
import jax.numpy as jnp
from jax import lax
from jax.experimental import pallas as pl
from jax.experimental.pallas import tpu as pltpu
from jax.sharding import PartitionSpec as P

MESH = pl.DeviceIdType.MESH
BF = jnp.bfloat16
F32 = jnp.float32
CORES = 2
WINDOW = 128
EPS = 1e-06


def mm(a, b):
    return jnp.dot(a, b, preferred_element_type=F32)


def mm_nt(a, b):
    return lax.dot_general(a, b, (((1,), (1,)), ((), ())), preferred_element_type=F32)


def mm_tn(a, b):
    return lax.dot_general(a, b, (((0,), (0,)), ((), ())), preferred_element_type=F32)


def iota(shape, dim):
    return lax.broadcasted_iota(jnp.int32, shape, dim)


def layer(
    dims,
    q_hbm,
    kt_hbm,
    vt_hbm,
    sink_ref,
    wo_hbm,
    res_ref,
    gain_ref,
    ids_ref,
    rw_ref,
    wg_hbm,
    wu_hbm,
    wd_hbm,
    out_ref,
    qv,
    kv,
    wo,
    wg,
    wu,
    wd,
    att,
    s2,
    r2,
    sp,
    sm,
    rp,
    rm,
    acc,
    stream,
    normed,
    own_a,
    ring,
    meta,
    table,
    place,
    sel,
    xin,
    yout,
    zin,
    ret,
    cbuf,
    load_sem,
    halo_sem,
    rs_send,
    rs_recv,
    d_send,
    d_recv,
    m_send,
    m_recv,
    p_send,
    p_recv,
    y_send,
    y_recv,
    b_send,
    b_recv,
):
    T, D, Z, TP, SP, CAP, HEADS, HD = dims
    PL = TP * CORES
    CH = PL * CAP
    HALF = D // 2
    HOPS = (Z // 2, Z // 2 - 1)
    PAIRS = Z // 4
    GR = 4 * CAP

    s = lax.axis_index("sp")
    x = lax.axis_index("tp")
    z = lax.div(s, CORES)
    c = lax.rem(s, CORES)
    me = c * TP + x
    step_a = 1 - 2 * c + Z
    z_next = (lax.rem(z + step_a, Z), lax.rem(z + 2 * Z - step_a, Z))

    def chip(zz):
        return {"sp": zz * CORES + c, "tp": x}

    ahead = (chip(z_next[0]), chip(z_next[1]))
    behind = (ahead[1], ahead[0])

    def to_x(k):
        return {"sp": s, "tp": lax.rem(x + k + TP, TP)}

    def peer(k):
        cc = lax.rem(c + k // TP, CORES)
        return {"sp": z * CORES + cc, "tp": lax.rem(x + k % TP, TP)}

    def peer_rank(k):
        return lax.rem(c + k // TP, CORES) * TP + lax.rem(x + k % TP, TP)

    def from_rank(k):
        return lax.rem(c + CORES - k // TP, CORES) * TP + lax.rem(x + TP - k % TP, TP)

    s_after = {"sp": lax.rem(s + 1, SP), "tp": x}
    s_before = {"sp": lax.rem(s + SP - 1, SP), "tp": x}

    loads = [
        pltpu.make_async_copy(q_hbm, qv, load_sem.at[0]),
        pltpu.make_async_copy(wo_hbm, wo, load_sem.at[1]),
        pltpu.make_async_copy(wg_hbm.at[0], wg, load_sem.at[2]),
        pltpu.make_async_copy(wu_hbm.at[0], wu, load_sem.at[3]),
        pltpu.make_async_copy(wd_hbm.at[0], wd, load_sem.at[4]),
    ]
    kv_loads = []
    for b in range(TP):
        cols = pl.ds(b * T, T)
        kv_loads.append(
            pltpu.make_async_copy(kt_hbm.at[:, cols], kv.at[b + 1, pl.ds(0, HD)], load_sem.at[5 + b])
        )
        kv_loads.append(
            pltpu.make_async_copy(
                vt_hbm.at[:, cols], kv.at[b + 1, pl.ds(HD, HD)], load_sem.at[5 + TP + b]
            )
        )
    for copy in kv_loads[::-1]:
        copy.start()
    loads[0].start()
    loads[1].start()

    barrier = pltpu.get_barrier_semaphore()
    greeted = [ahead[0], ahead[1], s_after, s_before] + [peer(k) for k in range(1, PL)]
    for device in greeted:
        pl.semaphore_signal(barrier, inc=1, device_id=device, device_id_type=MESH)
    for copy in kv_loads:
        copy.wait()
    pl.semaphore_wait(barrier, len(greeted))

    halo = pltpu.make_async_remote_copy(
        src_ref=kv.at[TP],
        dst_ref=kv.at[0],
        send_sem=halo_sem.at[0],
        recv_sem=halo_sem.at[1],
        device_id=s_after,
        device_id_type=MESH,
    )
    halo.start()
    for copy in loads[2:]:
        copy.start()

    row_i = iota((T, 2 * T), 0)
    col_j = iota((T, 2 * T), 1)

    def attend(b, slot):
        first = jnp.where(s * TP + b == 0, T, 0)
        allowed = (col_j > row_i) & (col_j <= row_i + T) & (col_j >= first)
        rows = pl.ds(pl.multiple_of(b * T, T), T)
        low = kv[b].astype(F32)
        high = kv[b + 1].astype(F32)
        both = jnp.concatenate([low, high], axis=1)
        kt, vt = both[:HD], both[HD:]
        none = jnp.zeros((HD, 2 * T), F32)
        keys = (jnp.concatenate([kt, none], 0).astype(BF), jnp.concatenate([none, kt], 0).astype(BF))
        values = (jnp.concatenate([vt, none], 0).astype(BF), jnp.concatenate([none, vt], 0).astype(BF))
        for pair in range(HEADS // 2):
            lanes = pl.ds(pair * 2 * HD, 2 * HD)
            query = qv[rows, lanes]
            total = None
            for side in range(2):
                sink = sink_ref[pair * 2 + side]
                score = mm(query, keys[side]) * (HD ** (-0.5))
                score = jnp.where(allowed, score, -jnp.inf)
                top = jnp.maximum(jnp.max(score, axis=1, keepdims=True), sink)
                grown = jnp.exp(score - top)
                weight = jnp.sum(grown, axis=1, keepdims=True) + jnp.exp(sink - top)
                mixed = mm_nt(grown.astype(BF), values[side]) / weight
                total = mixed if total is None else total + mixed
            att[slot, :, lanes] = total.astype(BF)

    def rs_copy(src, dst, index, device):
        return pltpu.make_async_remote_copy(
            src_ref=src,
            dst_ref=dst,
            send_sem=rs_send.at[index],
            recv_sem=rs_recv.at[index],
            device_id=device,
            device_id_type=MESH,
        )

    def project(slot, half):
        return mm(att[slot], wo[:, pl.ds(half * HALF, HALF)])

    right, left = to_x(1), to_x(-1)
    loads[0].wait()
    halo.wait()
    attend(lax.rem(x + 2, TP), 0)
    loads[1].wait()
    copies = []
    for half, device in ((0, right), (1, left)):
        s2[half] = project(0, half).astype(BF)
        copy = rs_copy(s2.at[half], r2.at[half], half, device)
        copy.start()
        copies.append(copy)
    attend(lax.rem(x + 1, TP), 1)
    sp[1] = project(1, 1).astype(BF)
    send_p1 = rs_copy(sp.at[1], rp.at[1], 2, right)
    send_p1.start()
    attend(lax.rem(x + TP - 1, TP), 2)
    sm[0] = project(2, 0).astype(BF)
    send_m0 = rs_copy(sm.at[0], rm.at[0], 3, left)
    send_m0.start()
    copies[0].wait_recv()
    sp[0] = (project(1, 0) + r2[0].astype(F32)).astype(BF)
    send_p0 = rs_copy(sp.at[0], rp.at[0], 4, right)
    send_p0.start()
    copies[1].wait_recv()
    sm[1] = (project(2, 1) + r2[1].astype(F32)).astype(BF)
    send_m1 = rs_copy(sm.at[1], rm.at[1], 5, left)
    send_m1.start()
    attend(x, 3)
    for half in range(2):
        cols = pl.ds(half * HALF, HALF)
        acc[:, cols] = project(3, half) + res_ref[:, cols].astype(F32)

    E = Z * PL
    e_sub = iota((E, T), 0)
    t_lane = iota((E, T), 1)
    first_id = ids_ref[0:1, :]
    second_id = ids_ref[1:2, :]
    took0 = jnp.where(e_sub == first_id, 1.0, 0.0).astype(F32)
    took1 = jnp.where(e_sub == second_id, 1.0, 0.0).astype(F32)
    took = took0 + took1
    before = jnp.where(iota((T, T), 0) < iota((T, T), 1), 1.0, 0.0).astype(BF)
    rank = mm(took.astype(BF), before)
    weight_a = rw_ref[0:1, :]
    weight_b = rw_ref[1:2, :]
    whole = weight_a + weight_b
    share = took0 * (weight_a / whole) + took1 * (weight_b / whole)
    plane_bits = PL.bit_length() - 1
    e_plane = lax.shift_right_logical(e_sub, plane_bits)
    rel = (e_plane - z) * (1 - 2 * c) + 2 * Z
    rel = rel & (Z - 1)
    is_a = (rel >= 1) & (rel <= HOPS[0])
    dist = (
        jnp.where(is_a, rel, 0).astype(F32),
        jnp.where(rel > HOPS[0], Z - rel, 0).astype(F32),
    )
    t_sub = iota((T, T), 0)
    t_col = iota((T, T), 1)
    positions = []
    for way in range(2):
        far = jnp.max(took * dist[way], axis=0, keepdims=True)
        along = jnp.broadcast_to(far, (T, T))
        down = along.T
        ahead_of = (down > along) | ((down == along) & (t_sub < t_col))
        positions.append(jnp.sum(jnp.where(ahead_of, 1.0, 0.0), axis=0, keepdims=True))
    for way in range(2):
        place[way] = jnp.where(positions[way] == t_sub.astype(F32), 1.0, 0.0).astype(BF)
    slot_value = jnp.where(is_a, positions[0] + 1.0, positions[1] + (1.0 + T))
    hop_number = jnp.where(is_a, rel, jnp.where(rel > HOPS[0], Z - rel, HOPS[0]))
    base = (
        (e_sub & (PL - 1)) * GR
        + ((hop_number - 1) & 1) * (2 * CAP)
        + jnp.where(is_a, 0, CAP)
    )
    spread_t = jnp.zeros((E, T), F32)
    spread_w = jnp.zeros((E, T), F32)
    for r in range(CAP):
        here = took * jnp.where(rank == float(r), 1.0, 0.0)
        value_col = jnp.sum(here * slot_value, axis=1, keepdims=True)
        share_col = jnp.sum(here * share, axis=1, keepdims=True)
        hit = t_lane == base + r
        spread_t = spread_t + jnp.where(hit, value_col, 0.0)
        spread_w = spread_w + jnp.where(hit, share_col, 0.0)
    plane_of = jnp.where(
        lax.shift_right_logical(iota((Z, E), 1), plane_bits) == iota((Z, E), 0), 1.0, 0.0
    ).astype(BF)
    OWN = HOPS[0] - 1
    meta[OWN, 1, pl.ds(0, Z)] = mm(plane_of, spread_t.astype(BF)).astype(BF)
    meta[OWN, 1, pl.ds(Z, Z)] = mm(plane_of, spread_w.astype(BF)).astype(BF)

    def prefix(way, hop):
        return min(T, CH * (HOPS[way] - hop + 1)) if hop <= HOPS[way] else 0

    for way in range(2):
        for hop in range(1, HOPS[way] + 1):
            n = prefix(way, hop)
            if n < T:
                ring[hop - 1, way, pl.ds(n, T - n)] = jnp.zeros((T - n, D), BF)

    send_p1.wait_recv()
    send_p0.wait_recv()
    send_m0.wait_recv()
    send_m1.wait_recv()
    ROWS = 32
    for r in range(T // ROWS):
        rows = pl.ds(r * ROWS, ROWS)
        square = jnp.zeros((ROWS, 1), F32)
        for half in range(2):
            cols = pl.ds(half * HALF, HALF)
            total = acc[rows, cols] + rp[half, rows].astype(F32) + rm[half, rows].astype(F32)
            kept = total.astype(BF)
            stream[rows, cols] = kept
            wide = kept.astype(F32)
            square = square + jnp.sum(wide * wide, axis=1, keepdims=True)
        scale = lax.rsqrt(square * (1.0 / D) + EPS)
        for half in range(2):
            cols = pl.ds(half * HALF, HALF)
            wide = stream[rows, cols].astype(F32)
            normed[rows, cols] = (wide * scale * gain_ref[:, cols]).astype(BF)

    def d_index(way, hop, j):
        return (way * HOPS[0] + hop - 1) * (T // CH) + j

    def packet_copy(way, hop, j):
        rows = pl.ds(j * CH, CH)
        if hop == 1:
            src = own_a.at[rows] if way == 0 else ring.at[OWN, 1, rows]
        else:
            src = ring.at[hop - 2, way, rows]
        index = d_index(way, hop, j)
        return pltpu.make_async_remote_copy(
            src_ref=src,
            dst_ref=ring.at[hop - 1, way, rows],
            send_sem=d_send.at[index],
            recv_sem=d_recv.at[index],
            device_id=ahead[way],
            device_id_type=MESH,
        )

    def meta_copy(way, hop):
        src = meta.at[OWN, 1] if hop == 1 else meta.at[hop - 2, way]
        index = way * HOPS[0] + hop - 1
        return pltpu.make_async_remote_copy(
            src_ref=src,
            dst_ref=meta.at[hop - 1, way],
            send_sem=m_send.at[index],
            recv_sem=m_recv.at[index],
            device_id=ahead[way],
            device_id_type=MESH,
        )

    for way in range(2):
        meta_copy(way, 1).start()
    for j in range(T // CH):
        rows = pl.ds(j * CH, CH)
        own_a[rows] = mm(place[0, rows], normed[...]).astype(BF)
        ring[OWN, 1, rows] = mm(place[1, rows], normed[...]).astype(BF)
        for way in range(2):
            packet_copy(way, 1, j).start()

    def pair_table(p):
        picked_t = jnp.zeros((1, T), F32)
        picked_w = jnp.zeros((1, T), F32)
        sub = iota((Z, T), 0)
        lane = iota((1, T), 1)
        for side in range(2):
            hop = 2 * p + 1 + side
            for way in range(2):
                known = meta[hop - 1, way].astype(F32)
                mine = sub == z
                picked_t = picked_t + jnp.sum(jnp.where(mine, known[:Z], 0.0), axis=0, keepdims=True)
                picked_w = picked_w + jnp.sum(jnp.where(mine, known[Z:], 0.0), axis=0, keepdims=True)
        late = (lane & (2 * CAP)) != 0
        picked_t = picked_t + jnp.where(late & (picked_t > 0.0), 2.0 * T, 0.0)
        table[p, 0:1] = picked_t
        table[p, 1:2] = picked_w

    def chosen(p):
        return (iota((4 * T, T), 0) + 1).astype(F32) == table[p, 0:1]

    def plane_copy(buffer_from, buffer_to, sends, recvs, p, k):
        index = p * PL + k
        rank_to = pl.ds(pl.multiple_of(peer_rank(k) * GR, GR), GR)
        rank_me = pl.ds(pl.multiple_of(me * GR, GR), GR)
        return pltpu.make_async_remote_copy(
            src_ref=buffer_from.at[p, rank_to],
            dst_ref=buffer_to.at[p, rank_me],
            send_sem=sends.at[index],
            recv_sem=recvs.at[index],
            device_id=peer(k),
            device_id_type=MESH,
        )

    def plane_wait(buffer_from, buffer_to, sends, recvs, p, k):
        index = p * PL + k
        rank_from = pl.ds(pl.multiple_of(from_rank(k) * GR, GR), GR)
        pltpu.make_async_remote_copy(
            src_ref=buffer_from.at[p, rank_from],
            dst_ref=buffer_to.at[p, rank_from],
            send_sem=sends.at[index],
            recv_sem=recvs.at[index],
            device_id=peer(k),
            device_id_type=MESH,
        ).wait_recv()

    mine_rows = pl.ds(pl.multiple_of(me * GR, GR), GR)
    COLS = 512

    def select(p):
        pair_table(p)
        hot = jnp.where(chosen(p), 1.0, 0.0).astype(BF)
        for n in range(D // COLS):
            cols = pl.ds(n * COLS, COLS)
            rows = ring[pl.ds(2 * p, 2), :, :, cols].reshape(4 * T, COLS)
            sel[p, :, cols] = mm_tn(hot, rows).astype(BF)
        for k in range(1, PL):
            plane_copy(sel, xin, p_send, p_recv, p, k).start()
        xin[p, mine_rows] = sel[p, mine_rows]

    def experts(p):
        for k in range(1, PL):
            plane_wait(sel, xin, p_send, p_recv, p, k)
        rows = xin[p]
        gate = mm(rows, wg[...])
        upward = mm(rows, wu[...])
        hidden = (gate / (1.0 + jnp.exp(-gate)) * upward).astype(BF)
        for n in range(D // COLS):
            cols = pl.ds(n * COLS, COLS)
            yout[p, :, cols] = mm(hidden, wd[:, cols]).astype(BF)
        for k in range(1, PL):
            plane_copy(yout, zin, y_send, y_recv, p, k).start()
        zin[p, mine_rows] = yout[p, mine_rows]

    for copy in loads[2:]:
        copy.wait()
    for hop in range(1, HOPS[0] + 1):
        for way in range(2):
            if hop <= HOPS[way]:
                meta_copy(way, hop).wait_recv()
                if hop < HOPS[way]:
                    meta_copy(way, hop + 1).start()
        for j in range(T // CH):
            for way in range(2):
                if j * CH < prefix(way, hop):
                    packet_copy(way, hop, j).wait_recv()
                if j * CH < prefix(way, hop + 1):
                    packet_copy(way, hop + 1, j).start()
        if hop % 2 == 0:
            p = hop // 2 - 1
            select(p)
            if p > 0:
                experts(p - 1)
    experts(PAIRS - 1)

    def back_copy(way, hop, j):
        rows = pl.ds(j * CH, CH)
        index = d_index(way, hop, j)
        return pltpu.make_async_remote_copy(
            src_ref=ret.at[hop, way, rows],
            dst_ref=ret.at[hop - 1, way, rows],
            send_sem=b_send.at[index],
            recv_sem=b_recv.at[index],
            device_id=behind[way],
            device_id_type=MESH,
        )

    def weighted(hop, way, n):
        p, side = (hop - 1) // 2, (hop - 1) % 2
        at = (side * 2 + way) * T
        hit = (iota((n, T), 0) + (at + 1)).astype(F32) == table[p, 0:1]
        mix = jnp.where(hit, table[p, 1:2], 0.0).astype(BF)
        for half in range(2):
            cols = pl.ds(half * HALF, HALF)
            cbuf[way, pl.ds(0, n), cols] = mm(mix, zin[p, :, cols])

    for hop in range(HOPS[0], 0, -1):
        if hop % 2 == 0:
            p = hop // 2 - 1
            for k in range(1, PL):
                plane_wait(yout, zin, y_send, y_recv, p, k)
        if hop == HOPS[0]:
            weighted(hop, 1, T)
            acc[...] = cbuf[1]
        for way in range(2):
            if hop <= HOPS[way]:
                weighted(hop, way, prefix(way, hop))
        for j in range(T // CH):
            rows = pl.ds(j * CH, CH)
            for way in range(2):
                if j * CH >= prefix(way, hop):
                    continue
                part = cbuf[way, rows]
                if j * CH < prefix(way, hop + 1):
                    back_copy(way, hop + 1, j).wait_recv()
                    part = part + ret[hop, way, rows].astype(F32)
                ret[hop, way, rows] = part.astype(BF)
                back_copy(way, hop, j).start()

    for j in range(T // CH):
        rows = pl.ds(j * CH, CH)
        for way in range(2):
            back_copy(way, 1, j).wait_recv()
        ret[0, 1, rows] = (ret[0, 1, rows].astype(F32) + acc[rows]).astype(BF)
    unsort = place[...].reshape(2 * T, T)
    for n in range(D // COLS):
        cols = pl.ds(n * COLS, COLS)
        came = ret[0, :, :, cols].reshape(2 * T, COLS)
        out_ref[:, cols] = (stream[:, cols].astype(F32) + mm_tn(unsort, came)).astype(BF)

    for copy in copies + [send_p1, send_m0, send_p0, send_m1]:
        copy.wait_send()
    for way in range(2):
        for hop in range(1, HOPS[way] + 1):
            meta_copy(way, hop).wait_send()
            for j in range(T // CH):
                if j * CH < prefix(way, hop):
                    packet_copy(way, hop, j).wait_send()
                    back_copy(way, hop, j).wait_send()
    for p in range(PAIRS):
        for k in range(1, PL):
            plane_copy(sel, xin, p_send, p_recv, p, k).wait_send()
            plane_copy(yout, zin, y_send, y_recv, p, k).wait_send()


def solution(mesh):
    sp_count = mesh.shape["sp"]
    tp_count = mesh.shape["tp"]

    def on_device(
        queries,
        key_heads,
        value_heads,
        sink_logit,
        out_weight,
        residual,
        norm_gain,
        expert_ids,
        route_weights,
        gate_weight,
        up_weight,
        down_weight,
    ):
        T, D = residual.shape
        HD = key_heads.shape[2]
        HEADS = queries.shape[1] // HD
        FF = gate_weight.shape[2]
        Z = sp_count // CORES
        PL = tp_count * CORES
        top_k = expert_ids.shape[1]
        CAP = max(2, 2 * top_k * T // (sp_count * tp_count))
        PAIRS = Z // 4
        GR = 4 * CAP
        HOP = Z // 2
        keys_t = jnp.transpose(key_heads, (1, 2, 0)).reshape(HD, -1)
        values_t = jnp.transpose(value_heads, (1, 2, 0)).reshape(HD, -1)
        dma = pltpu.SemaphoreType.DMA
        vm = pltpu.VMEM
        any_space = pl.BlockSpec(memory_space=pl.ANY)
        in_vmem = pl.BlockSpec(memory_space=pltpu.VMEM)
        dims = (T, D, Z, tp_count, sp_count, CAP, HEADS, HD)
        chunks = T // (PL * CAP)
        return pl.pallas_call(
            functools.partial(layer, dims),
            out_shape=jax.ShapeDtypeStruct((T, D), BF),
            in_specs=[
                any_space,
                any_space,
                any_space,
                pl.BlockSpec(memory_space=pltpu.SMEM),
                any_space,
                in_vmem,
                in_vmem,
                in_vmem,
                in_vmem,
                any_space,
                any_space,
                any_space,
            ],
            out_specs=in_vmem,
            scratch_shapes=[
                vm(queries.shape, BF),
                vm((tp_count + 1, 2 * HD, T), BF),
                vm(out_weight.shape, BF),
                vm((D, FF), BF),
                vm((D, FF), BF),
                vm((FF, D), BF),
                vm((4, T, HEADS * HD), BF),
                vm((2, T, D // 2), BF),
                vm((2, T, D // 2), BF),
                vm((2, T, D // 2), BF),
                vm((2, T, D // 2), BF),
                vm((2, T, D // 2), BF),
                vm((2, T, D // 2), BF),
                vm((T, D), F32),
                vm((T, D), BF),
                vm((T, D), BF),
                vm((T, D), BF),
                vm((HOP, 2, T, D), BF),
                vm((HOP, 2, 2 * Z, T), BF),
                vm((PAIRS, 8, T), F32),
                vm((2, T, T), BF),
                vm((PAIRS, PL * GR, D), BF),
                vm((PAIRS, PL * GR, D), BF),
                vm((PAIRS, PL * GR, D), BF),
                vm((PAIRS, PL * GR, D), BF),
                vm((HOP + 1, 2, T, D), BF),
                vm((2, T, D), F32),
                dma((5 + 2 * tp_count,)),
                dma((2,)),
                dma((6,)),
                dma((6,)),
                dma((2 * HOP * chunks,)),
                dma((2 * HOP * chunks,)),
                dma((2 * HOP,)),
                dma((2 * HOP,)),
                dma((PAIRS * PL,)),
                dma((PAIRS * PL,)),
                dma((PAIRS * PL,)),
                dma((PAIRS * PL,)),
                dma((2 * HOP * chunks,)),
                dma((2 * HOP * chunks,)),
            ],
            compiler_params=pltpu.CompilerParams(
                collective_id=0, has_side_effects=True, vmem_limit_bytes=62 * 1024 * 1024
            ),
        )(
            queries,
            keys_t,
            values_t,
            sink_logit,
            out_weight,
            residual,
            norm_gain.reshape(1, D),
            expert_ids.T,
            route_weights.T,
            gate_weight,
            up_weight,
            down_weight,
        )

    return jax.shard_map(
        on_device,
        mesh=mesh,
        in_specs=(
            P(("grp", "sp"), "tp"),
            P(("grp", "sp"), "tp", None),
            P(("grp", "sp"), "tp", None),
            P("tp"),
            P("tp", None),
            P(("grp", "sp", "tp"), None),
            P(),
            P(("grp", "sp", "tp"), None),
            P(("grp", "sp", "tp"), None),
            P(("sp", "tp"), None, None),
            P(("sp", "tp"), None, None),
            P(("sp", "tp"), None, None),
        ),
        out_specs=P(("grp", "sp", "tp"), None),
        check_vma=False,
    )
```

time: 356 us -> 221 us (0.62)
  Pallas kernels: 0 us -> 218 us
  waiting for transfers between devices: 152 us -> 0 us
  blocking collectives: 114 us -> 0 us
  local copies, waits for them, and re-layouts: 36.3 us -> 1.88 us
  starting transfers between devices: 20.8 us -> 0 us
  matrix products: 16.7 us -> 0 us
  other arithmetic: 15.5 us -> 0 us
    pallas_call x0 -> x1, Pallas kernels: none -> 218 us  [on_device(): pl.pallas_call(functools.partial(layer, dims), out_shape=jax.ShapeDtypeSt...]
    all_to_all x2 -> x0, waiting for transfers between devices: 139 us -> none  [the longest x1 97.7 us: on_device(): lax.all_to_all(results, ('sp', 'tp'), split_axis=0, concat_axis=0, tiled=...]
    all_to_all x1 -> x0, blocking collectives: 114 us -> none  [on_device(): lax.all_to_all(outbox, ('sp', 'tp'), split_axis=0, concat_axis=0, tiled=T...]
    dot_general x5 -> x0, matrix products: 16.7 us -> none  [the longest x1 6.9 us: on_device(): jnp.dot(expert_hidden, w_down_own, preferred_element_type=jnp.float32)]
    all_to_all x2 -> x0, starting transfers between devices: 15.1 us -> none  [the longest x1 10 us: on_device(): lax.all_to_all(results, ('sp', 'tp'), split_axis=0, concat_axis=0, tiled=...]
    ppermute x1 -> x0, waiting for transfers between devices: 12.9 us -> none  [from_behind(): lax.ppermute(value, axis, [(source, source + steps) for source in range(i...]
    gather x3 -> x0, local copies, waits for them, and re-layouts: 12.7 us -> none  [the longest x2 7.47 us: on_device(): normed[token_in_slot]]
    reshape x3 -> x0, local copies, waits for them, and re-layouts: 12 us -> none  [the longest x1 4.11 us: on_device(): results = expert_rows.reshape(arrived.shape)]
  transfers between devices with their start and end apart: 3 -> 0, of which waited for: 3 -> 0; matrix products, arithmetic and copies ran while one was open for 2% -> 0% of each run, Pallas kernels for 0% -> 0%
where the time goes in v1:
time: 221 us; the launch traced here: 220 us
  Pallas kernels  218 us (99%)
    pallas_call x1, Pallas kernels, on_device(): pl.pallas_call(functools.partial(layer, dims), out_shape=jax.ShapeDtypeSt...  218 us

profile of v1, /device:TPU:33, one launch (start us, length us, event | category | flops | bytes accessed | tf_op | source)
XLA Modules:
  0.0 219.8 jit_solution(2621009364706603710)
XLA Ops:
  0.0 217.9 %shard_map.118 = bf16[128,2048]{1,0:T(8,128)(2,1)} custom-call(bf16[512,512]{1,0:T(8,128)(2,1)} %q_hbm.1, bf16[64,512]{1,0:T(8,128)(2,1)} %bitcast.9, bf16[64,512]{1,0:T(8,128)(2,1)} %bitcast.10, f32[8]{0:T(128)} %sink_ref.1, bf16[512,2048]{1,0:T(8,128)(2,1)} %wo_hbm.1, bf16[128,2048]{1,0:T(8,128)(2,1)} %res_ref.1, f32[1,2048]{1,0:T(1,128)} %bitcast.11, ...), custom_call_target="tpu_custom_call" | custom-call | tf_op jit(solution)/shard_map/pallas_call | solution.py:574
  217.9 1.9 copy.14

commit v2 on v1

--- a/solution.py
+++ b/solution.py
@@ -89,12 +89,13 @@
     b_recv,
 ):
     T, D, Z, TP, SP, CAP, HEADS, HD = dims
+    LAST = Z // 2
     PL = TP * CORES
     CH = PL * CAP
     HALF = D // 2
     HOPS = (Z // 2, Z // 2 - 1)
-    PAIRS = Z // 4
-    GR = 4 * CAP
+    GR = 2 * CAP
+    SEL = PL * GR
 
     s = lax.axis_index("sp")
     x = lax.axis_index("tp")
@@ -144,18 +145,14 @@
                 vt_hbm.at[:, cols], kv.at[b + 1, pl.ds(HD, HD)], load_sem.at[5 + TP + b]
             )
         )
+    barrier = pltpu.get_barrier_semaphore()
+    greeted = [ahead[0], ahead[1], s_after, s_before] + [peer(k) for k in range(1, PL)]
+    for device in greeted:
+        pl.semaphore_signal(barrier, inc=1, device_id=device, device_id_type=MESH)
     for copy in kv_loads[::-1]:
         copy.start()
     loads[0].start()
     loads[1].start()
-
-    barrier = pltpu.get_barrier_semaphore()
-    greeted = [ahead[0], ahead[1], s_after, s_before] + [peer(k) for k in range(1, PL)]
-    for device in greeted:
-        pl.semaphore_signal(barrier, inc=1, device_id=device, device_id_type=MESH)
-    for copy in kv_loads:
-        copy.wait()
-    pl.semaphore_wait(barrier, len(greeted))
 
     halo = pltpu.make_async_remote_copy(
         src_ref=kv.at[TP],
@@ -165,9 +162,6 @@
         device_id=s_after,
         device_id_type=MESH,
     )
-    halo.start()
-    for copy in loads[2:]:
-        copy.start()
 
     row_i = iota((T, 2 * T), 0)
     col_j = iota((T, 2 * T), 1)
@@ -212,36 +206,45 @@
         return mm(att[slot], wo[:, pl.ds(half * HALF, HALF)])
 
     right, left = to_x(1), to_x(-1)
+    for copy in kv_loads:
+        copy.wait()
     loads[0].wait()
+    attend(1, 1)
+    pl.semaphore_wait(barrier, len(greeted))
+    halo.start()
+    for copy in loads[2:]:
+        copy.start()
+    for b in range(2, TP):
+        attend(b, b)
+    loads[1].wait()
     halo.wait()
-    attend(lax.rem(x + 2, TP), 0)
-    loads[1].wait()
+    attend(0, 0)
+    far, after, prior = lax.rem(x + 2, TP), lax.rem(x + 1, TP), lax.rem(x + TP - 1, TP)
     copies = []
     for half, device in ((0, right), (1, left)):
-        s2[half] = project(0, half).astype(BF)
+        s2[half] = project(far, half).astype(BF)
         copy = rs_copy(s2.at[half], r2.at[half], half, device)
         copy.start()
         copies.append(copy)
-    attend(lax.rem(x + 1, TP), 1)
-    sp[1] = project(1, 1).astype(BF)
+    sp[1] = project(after, 1).astype(BF)
     send_p1 = rs_copy(sp.at[1], rp.at[1], 2, right)
     send_p1.start()
-    attend(lax.rem(x + TP - 1, TP), 2)
-    sm[0] = project(2, 0).astype(BF)
+    sm[0] = project(prior, 0).astype(BF)
     send_m0 = rs_copy(sm.at[0], rm.at[0], 3, left)
     send_m0.start()
+    for half in range(2):
+        cols = pl.ds(half * HALF, HALF)
+        acc[:, cols] = project(x, half) + res_ref[:, cols].astype(F32)
+    early = project(after, 0)
     copies[0].wait_recv()
-    sp[0] = (project(1, 0) + r2[0].astype(F32)).astype(BF)
+    sp[0] = (early + r2[0].astype(F32)).astype(BF)
     send_p0 = rs_copy(sp.at[0], rp.at[0], 4, right)
     send_p0.start()
+    early = project(prior, 1)
     copies[1].wait_recv()
-    sm[1] = (project(2, 1) + r2[1].astype(F32)).astype(BF)
+    sm[1] = (early + r2[1].astype(F32)).astype(BF)
     send_m1 = rs_copy(sm.at[1], rm.at[1], 5, left)
     send_m1.start()
-    attend(x, 3)
-    for half in range(2):
-        cols = pl.ds(half * HALF, HALF)
-        acc[:, cols] = project(3, half) + res_ref[:, cols].astype(F32)
 
     E = Z * PL
     e_sub = iota((E, T), 0)
@@ -278,12 +281,7 @@
     for way in range(2):
         place[way] = jnp.where(positions[way] == t_sub.astype(F32), 1.0, 0.0).astype(BF)
     slot_value = jnp.where(is_a, positions[0] + 1.0, positions[1] + (1.0 + T))
-    hop_number = jnp.where(is_a, rel, jnp.where(rel > HOPS[0], Z - rel, HOPS[0]))
-    base = (
-        (e_sub & (PL - 1)) * GR
-        + ((hop_number - 1) & 1) * (2 * CAP)
-        + jnp.where(is_a, 0, CAP)
-    )
+    base = (e_sub & (PL - 1)) * GR + jnp.where(is_a, 0, CAP)
     spread_t = jnp.zeros((E, T), F32)
     spread_w = jnp.zeros((E, T), F32)
     for r in range(CAP):
@@ -367,102 +365,77 @@
         rows = pl.ds(j * CH, CH)
         own_a[rows] = mm(place[0, rows], normed[...]).astype(BF)
         ring[OWN, 1, rows] = mm(place[1, rows], normed[...]).astype(BF)
-        for way in range(2):
-            packet_copy(way, 1, j).start()
-
-    def pair_table(p):
+        if j < 2:
+            for way in range(2):
+                packet_copy(way, 1, j).start()
+
+    def hop_table(hop):
         picked_t = jnp.zeros((1, T), F32)
         picked_w = jnp.zeros((1, T), F32)
-        sub = iota((Z, T), 0)
-        lane = iota((1, T), 1)
-        for side in range(2):
-            hop = 2 * p + 1 + side
-            for way in range(2):
-                known = meta[hop - 1, way].astype(F32)
-                mine = sub == z
-                picked_t = picked_t + jnp.sum(jnp.where(mine, known[:Z], 0.0), axis=0, keepdims=True)
-                picked_w = picked_w + jnp.sum(jnp.where(mine, known[Z:], 0.0), axis=0, keepdims=True)
-        late = (lane & (2 * CAP)) != 0
-        picked_t = picked_t + jnp.where(late & (picked_t > 0.0), 2.0 * T, 0.0)
-        table[p, 0:1] = picked_t
-        table[p, 1:2] = picked_w
-
-    def chosen(p):
-        return (iota((4 * T, T), 0) + 1).astype(F32) == table[p, 0:1]
-
-    def plane_copy(buffer_from, buffer_to, sends, recvs, p, k):
-        index = p * PL + k
-        rank_to = pl.ds(pl.multiple_of(peer_rank(k) * GR, GR), GR)
-        rank_me = pl.ds(pl.multiple_of(me * GR, GR), GR)
+        mine = iota((Z, T), 0) == z
+        for way in range(2):
+            known = meta[hop - 1, way].astype(F32)
+            picked_t = picked_t + jnp.sum(jnp.where(mine, known[:Z], 0.0), axis=0, keepdims=True)
+            picked_w = picked_w + jnp.sum(jnp.where(mine, known[Z:], 0.0), axis=0, keepdims=True)
+        table[hop - 1, 0:1] = picked_t
+        table[hop - 1, 1:2] = picked_w
+
+    def plane_copy(buffer_from, buffer_to, sends, recvs, hop, k):
+        index = (hop - 1) * PL + k
         return pltpu.make_async_remote_copy(
-            src_ref=buffer_from.at[p, rank_to],
-            dst_ref=buffer_to.at[p, rank_me],
+            src_ref=buffer_from.at[hop - 1, peer_rank(k)],
+            dst_ref=buffer_to.at[hop - 1, me],
             send_sem=sends.at[index],
             recv_sem=recvs.at[index],
             device_id=peer(k),
             device_id_type=MESH,
         )
 
-    def plane_wait(buffer_from, buffer_to, sends, recvs, p, k):
-        index = p * PL + k
-        rank_from = pl.ds(pl.multiple_of(from_rank(k) * GR, GR), GR)
+    def plane_wait(buffer_from, buffer_to, sends, recvs, hop, k):
+        index = (hop - 1) * PL + k
         pltpu.make_async_remote_copy(
-            src_ref=buffer_from.at[p, rank_from],
-            dst_ref=buffer_to.at[p, rank_from],
+            src_ref=buffer_from.at[hop - 1, from_rank(k)],
+            dst_ref=buffer_to.at[hop - 1, from_rank(k)],
             send_sem=sends.at[index],
             recv_sem=recvs.at[index],
             device_id=peer(k),
             device_id_type=MESH,
         ).wait_recv()
 
-    mine_rows = pl.ds(pl.multiple_of(me * GR, GR), GR)
     COLS = 512
 
-    def select(p):
-        pair_table(p)
-        hot = jnp.where(chosen(p), 1.0, 0.0).astype(BF)
+    def select(hop):
+        hop_table(hop)
+        spot = (iota((2 * T, SEL), 0) + 1).astype(F32)
+        hot = jnp.where(spot == table[hop - 1, 0:1, 0:SEL], 1.0, 0.0).astype(BF)
         for n in range(D // COLS):
             cols = pl.ds(n * COLS, COLS)
-            rows = ring[pl.ds(2 * p, 2), :, :, cols].reshape(4 * T, COLS)
-            sel[p, :, cols] = mm_tn(hot, rows).astype(BF)
+            rows = ring[hop - 1, :, :, cols].reshape(2 * T, COLS)
+            sel[hop - 1, :, :, cols] = mm_tn(hot, rows).reshape(PL, GR, COLS).astype(BF)
         for k in range(1, PL):
-            plane_copy(sel, xin, p_send, p_recv, p, k).start()
-        xin[p, mine_rows] = sel[p, mine_rows]
-
-    def experts(p):
-        for k in range(1, PL):
-            plane_wait(sel, xin, p_send, p_recv, p, k)
-        rows = xin[p]
+            plane_copy(sel, xin, p_send, p_recv, hop, k).start()
+        xin[hop - 1, me] = sel[hop - 1, me]
+
+    def experts(*hops):
+        for hop in hops:
+            for k in range(1, PL):
+                plane_wait(sel, xin, p_send, p_recv, hop, k)
+        rows = jnp.concatenate(
+            [xin[hop - 1].astype(F32).reshape(SEL, D).astype(BF) for hop in hops], axis=0
+        )
         gate = mm(rows, wg[...])
         upward = mm(rows, wu[...])
         hidden = (gate / (1.0 + jnp.exp(-gate)) * upward).astype(BF)
         for n in range(D // COLS):
             cols = pl.ds(n * COLS, COLS)
-            yout[p, :, cols] = mm(hidden, wd[:, cols]).astype(BF)
-        for k in range(1, PL):
-            plane_copy(yout, zin, y_send, y_recv, p, k).start()
-        zin[p, mine_rows] = yout[p, mine_rows]
-
-    for copy in loads[2:]:
-        copy.wait()
-    for hop in range(1, HOPS[0] + 1):
-        for way in range(2):
-            if hop <= HOPS[way]:
-                meta_copy(way, hop).wait_recv()
-                if hop < HOPS[way]:
-                    meta_copy(way, hop + 1).start()
-        for j in range(T // CH):
-            for way in range(2):
-                if j * CH < prefix(way, hop):
-                    packet_copy(way, hop, j).wait_recv()
-                if j * CH < prefix(way, hop + 1):
-                    packet_copy(way, hop + 1, j).start()
-        if hop % 2 == 0:
-            p = hop // 2 - 1
-            select(p)
-            if p > 0:
-                experts(p - 1)
-    experts(PAIRS - 1)
+            product = mm(hidden, wd[:, cols])
+            for i, hop in enumerate(hops):
+                part = product[i * SEL : (i + 1) * SEL]
+                yout[hop - 1, :, :, cols] = part.reshape(PL, GR, COLS).astype(BF)
+        for hop in hops:
+            for k in range(1, PL):
+                plane_copy(yout, zin, y_send, y_recv, hop, k).start()
+            zin[hop - 1, me] = yout[hop - 1, me]
 
     def back_copy(way, hop, j):
         rows = pl.ds(j * CH, CH)
@@ -476,37 +449,75 @@
             device_id_type=MESH,
         )
 
-    def weighted(hop, way, n):
-        p, side = (hop - 1) // 2, (hop - 1) % 2
-        at = (side * 2 + way) * T
-        hit = (iota((n, T), 0) + (at + 1)).astype(F32) == table[p, 0:1]
-        mix = jnp.where(hit, table[p, 1:2], 0.0).astype(BF)
-        for half in range(2):
-            cols = pl.ds(half * HALF, HALF)
-            cbuf[way, pl.ds(0, n), cols] = mm(mix, zin[p, :, cols])
-
-    for hop in range(HOPS[0], 0, -1):
-        if hop % 2 == 0:
-            p = hop // 2 - 1
-            for k in range(1, PL):
-                plane_wait(yout, zin, y_send, y_recv, p, k)
-        if hop == HOPS[0]:
-            weighted(hop, 1, T)
+    def weighted(hop, ways):
+        for k in range(1, PL):
+            plane_wait(yout, zin, y_send, y_recv, hop, k)
+        mixes = []
+        for way, n in ways:
+            spot = (iota((n, SEL), 0) + (way * T + 1)).astype(F32)
+            hit = spot == table[hop - 1, 0:1, 0:SEL]
+            mixes.append(jnp.where(hit, table[hop - 1, 1:2, 0:SEL], 0.0).astype(BF))
+        for n in range(D // COLS):
+            cols = pl.ds(n * COLS, COLS)
+            rows = zin[hop - 1, :, :, cols].astype(F32).reshape(SEL, COLS).astype(BF)
+            for (way, count), mix in zip(ways, mixes):
+                cbuf[way, pl.ds(0, count), cols] = mm(mix, rows)
+
+    def send_back(hop):
+        if hop == LAST:
+            weighted(hop, [(0, prefix(0, hop)), (1, T)])
             acc[...] = cbuf[1]
-        for way in range(2):
-            if hop <= HOPS[way]:
-                weighted(hop, way, prefix(way, hop))
-        for j in range(T // CH):
-            rows = pl.ds(j * CH, CH)
+        else:
+            weighted(hop, [(way, prefix(way, hop)) for way in range(2)])
+        for i in range(T // CH):
             for way in range(2):
-                if j * CH >= prefix(way, hop):
+                j = prefix(way, hop) // CH - 1 - i
+                if j < 0:
                     continue
+                rows = pl.ds(j * CH, CH)
                 part = cbuf[way, rows]
                 if j * CH < prefix(way, hop + 1):
                     back_copy(way, hop + 1, j).wait_recv()
                     part = part + ret[hop, way, rows].astype(F32)
                 ret[hop, way, rows] = part.astype(BF)
                 back_copy(way, hop, j).start()
+
+    def pass_on(way, hop, j):
+        if j * CH < prefix(way, hop):
+            packet_copy(way, hop, j).wait_recv()
+        if j * CH < prefix(way, hop + 1):
+            packet_copy(way, hop + 1, j).start()
+
+    for copy in loads[2:]:
+        copy.wait()
+    for hop in range(1, LAST + 1):
+        for way in range(2):
+            if hop <= HOPS[way]:
+                meta_copy(way, hop).wait_recv()
+                if hop < HOPS[way]:
+                    meta_copy(way, hop + 1).start()
+        for j in range(2):
+            for way in range(2):
+                pass_on(way, hop, j)
+                if hop == HOPS[way] - 1:
+                    packet_copy(way, 1, 2 + j).start()
+    select(LAST)
+    select(LAST - 1)
+    for hop in range(1, LAST - 1):
+        for j in range(2, 4):
+            for way in range(2):
+                pass_on(way, hop, j)
+        select(hop)
+        if hop == 2:
+            experts(LAST, LAST - 1)
+        if hop == LAST - 3:
+            send_back(LAST)
+    send_back(LAST - 1)
+    experts(LAST - 2, LAST - 3)
+    experts(1, 2)
+    experts(3, 4)
+    for hop in range(LAST - 2, 0, -1):
+        send_back(hop)
 
     for j in range(T // CH):
         rows = pl.ds(j * CH, CH)
@@ -528,10 +539,10 @@
                 if j * CH < prefix(way, hop):
                     packet_copy(way, hop, j).wait_send()
                     back_copy(way, hop, j).wait_send()
-    for p in range(PAIRS):
+    for hop in range(1, LAST + 1):
         for k in range(1, PL):
-            plane_copy(sel, xin, p_send, p_recv, p, k).wait_send()
-            plane_copy(yout, zin, y_send, y_recv, p, k).wait_send()
+            plane_copy(sel, xin, p_send, p_recv, hop, k).wait_send()
+            plane_copy(yout, zin, y_send, y_recv, hop, k).wait_send()
 
 
 def solution(mesh):
@@ -560,8 +571,7 @@
         PL = tp_count * CORES
         top_k = expert_ids.shape[1]
         CAP = max(2, 2 * top_k * T // (sp_count * tp_count))
-        PAIRS = Z // 4
-        GR = 4 * CAP
+        GR = 2 * CAP
         HOP = Z // 2
         keys_t = jnp.transpose(key_heads, (1, 2, 0)).reshape(HD, -1)
         values_t = jnp.transpose(value_heads, (1, 2, 0)).reshape(HD, -1)
@@ -609,12 +619,12 @@
                 vm((T, D), BF),
                 vm((HOP, 2, T, D), BF),
                 vm((HOP, 2, 2 * Z, T), BF),
-                vm((PAIRS, 8, T), F32),
+                vm((HOP, 8, T), F32),
                 vm((2, T, T), BF),
-                vm((PAIRS, PL * GR, D), BF),
-                vm((PAIRS, PL * GR, D), BF),
-                vm((PAIRS, PL * GR, D), BF),
-                vm((PAIRS, PL * GR, D), BF),
+                vm((HOP, PL, GR, D), BF),
+                vm((HOP, PL, GR, D), BF),
+                vm((HOP, PL, GR, D), BF),
+                vm((HOP, PL, GR, D), BF),
                 vm((HOP + 1, 2, T, D), BF),
                 vm((2, T, D), F32),
                 dma((5 + 2 * tp_count,)),
@@ -625,10 +635,10 @@
                 dma((2 * HOP * chunks,)),
                 dma((2 * HOP,)),
                 dma((2 * HOP,)),
-                dma((PAIRS * PL,)),
-                dma((PAIRS * PL,)),
-                dma((PAIRS * PL,)),
-                dma((PAIRS * PL,)),
+                dma((HOP * PL,)),
+                dma((HOP * PL,)),
+                dma((HOP * PL,)),
+                dma((HOP * PL,)),
                 dma((2 * HOP * chunks,)),
                 dma((2 * HOP * chunks,)),
             ],

time: 221 us -> 205 us (0.928)
  Pallas kernels: 218 us -> 203 us
    pallas_call x1, Pallas kernels: 218 us -> 203 us  [on_device(): pl.pallas_call(functools.partial(layer, dims), out_shape=jax.ShapeDtypeSt...]
where the time goes in v2:
time: 205 us
  Pallas kernels  203 us (99%)
    pallas_call x1, Pallas kernels, on_device(): pl.pallas_call(functools.partial(layer, dims), out_shape=jax.ShapeDtypeSt...  203 us

profile of v2, /device:TPU:33, one launch (start us, length us, event | category | flops | bytes accessed | tf_op | source)
XLA Modules:
  0.0 204.6 jit_solution(8517226175849881466)
XLA Ops:
  0.0 202.8 %shard_map.118 = bf16[128,2048]{1,0:T(8,128)(2,1)} custom-call(bf16[512,512]{1,0:T(8,128)(2,1)} %q_hbm.1, bf16[64,512]{1,0:T(8,128)(2,1)} %bitcast.9, bf16[64,512]{1,0:T(8,128)(2,1)} %bitcast.10, f32[8]{0:T(128)} %sink_ref.1, bf16[512,2048]{1,0:T(8,128)(2,1)} %wo_hbm.1, bf16[128,2048]{1,0:T(8,128)(2,1)} %res_ref.1, f32[1,2048]{1,0:T(1,128)} %bitcast.11, ...), custom_call_target="tpu_custom_call" | custom-call | tf_op jit(solution)/shard_map/pallas_call | solution.py:584
  202.8 1.9 copy.14

commit v3 on v2

--- a/solution.py
+++ b/solution.py
@@ -29,6 +29,54 @@
 
 def iota(shape, dim):
     return lax.broadcasted_iota(jnp.int32, shape, dim)
+
+
+PIECE = 16
+
+
+def prefix_rows(hops, rows, share):
+    def prefix(way, hop):
+        return min(rows, share * (hops[way] - hop + 1)) if hop <= hops[way] else 0
+
+    return prefix
+
+
+def ring_order(prefix, rows, ready, latency=3.0, waiting=1):
+    queue, left, now, clock = ([], []), [0.0, 0.0], [None, None], 0.0
+    own = [list(range(rows // PIECE)) for _ in range(2)]
+    coming, events = [], []
+    while True:
+        for way in range(2):
+            while (
+                own[way]
+                and ready[own[way][0]] <= clock + 1e-6
+                and len(queue[way]) + (now[way] is not None) <= waiting
+            ):
+                piece = own[way].pop(0)
+                queue[way].append((piece, 1))
+                events.append((clock, "own", way, piece, 1))
+            if now[way] is None and queue[way]:
+                now[way], left[way] = queue[way].pop(0), 1.0
+        busy = [way for way in range(2) if now[way] is not None]
+        steps = [clock + left[way] * len(busy) for way in busy]
+        steps += [item[0] for item in coming]
+        steps += [ready[own[way][0]] for way in range(2) if own[way] and ready[own[way][0]] > clock]
+        if not steps:
+            return events
+        later = min(steps)
+        for way in busy:
+            left[way] -= (later - clock) / len(busy)
+        clock = later
+        for way in busy:
+            if left[way] < 1e-6:
+                coming.append((clock + latency, way) + now[way])
+                now[way] = None
+        coming.sort()
+        while coming and coming[0][0] <= clock + 1e-6:
+            _, way, piece, hop = coming.pop(0)
+            events.append((clock, "pass", way, piece, hop))
+            if piece * PIECE < prefix(way, hop + 1):
+                queue[way].append((piece, hop + 1))
 
 
 def layer(
@@ -298,9 +346,7 @@
     meta[OWN, 1, pl.ds(0, Z)] = mm(plane_of, spread_t.astype(BF)).astype(BF)
     meta[OWN, 1, pl.ds(Z, Z)] = mm(plane_of, spread_w.astype(BF)).astype(BF)
 
-    def prefix(way, hop):
-        return min(T, CH * (HOPS[way] - hop + 1)) if hop <= HOPS[way] else 0
-
+    prefix = prefix_rows(HOPS, T, CH)
     for way in range(2):
         for hop in range(1, HOPS[way] + 1):
             n = prefix(way, hop)
@@ -329,10 +375,10 @@
             normed[rows, cols] = (wide * scale * gain_ref[:, cols]).astype(BF)
 
     def d_index(way, hop, j):
-        return (way * HOPS[0] + hop - 1) * (T // CH) + j
+        return (way * HOPS[0] + hop - 1) * (T // PIECE) + j
 
     def packet_copy(way, hop, j):
-        rows = pl.ds(j * CH, CH)
+        rows = pl.ds(j * PIECE, PIECE)
         if hop == 1:
             src = own_a.at[rows] if way == 0 else ring.at[OWN, 1, rows]
         else:
@@ -365,9 +411,10 @@
         rows = pl.ds(j * CH, CH)
         own_a[rows] = mm(place[0, rows], normed[...]).astype(BF)
         ring[OWN, 1, rows] = mm(place[1, rows], normed[...]).astype(BF)
-        if j < 2:
+        if j == 0:
             for way in range(2):
-                packet_copy(way, 1, j).start()
+                for i in range(2):
+                    packet_copy(way, 1, i).start()
 
     def hop_table(hop):
         picked_t = jnp.zeros((1, T), F32)
@@ -438,7 +485,7 @@
             zin[hop - 1, me] = yout[hop - 1, me]
 
     def back_copy(way, hop, j):
-        rows = pl.ds(j * CH, CH)
+        rows = pl.ds(j * PIECE, PIECE)
         index = d_index(way, hop, j)
         return pltpu.make_async_remote_copy(
             src_ref=ret.at[hop, way, rows],
@@ -469,49 +516,60 @@
             acc[...] = cbuf[1]
         else:
             weighted(hop, [(way, prefix(way, hop)) for way in range(2)])
-        for i in range(T // CH):
+        for i in range(T // PIECE):
             for way in range(2):
-                j = prefix(way, hop) // CH - 1 - i
+                j = prefix(way, hop) // PIECE - 1 - i
                 if j < 0:
                     continue
-                rows = pl.ds(j * CH, CH)
+                rows = pl.ds(j * PIECE, PIECE)
                 part = cbuf[way, rows]
-                if j * CH < prefix(way, hop + 1):
+                if j * PIECE < prefix(way, hop + 1):
                     back_copy(way, hop + 1, j).wait_recv()
                     part = part + ret[hop, way, rows].astype(F32)
                 ret[hop, way, rows] = part.astype(BF)
                 back_copy(way, hop, j).start()
 
     def pass_on(way, hop, j):
-        if j * CH < prefix(way, hop):
+        if j * PIECE < prefix(way, hop):
             packet_copy(way, hop, j).wait_recv()
-        if j * CH < prefix(way, hop + 1):
+        if j * PIECE < prefix(way, hop + 1):
             packet_copy(way, hop + 1, j).start()
 
     for copy in loads[2:]:
         copy.wait()
-    for hop in range(1, LAST + 1):
-        for way in range(2):
-            if hop <= HOPS[way]:
-                meta_copy(way, hop).wait_recv()
-                if hop < HOPS[way]:
-                    meta_copy(way, hop + 1).start()
-        for j in range(2):
-            for way in range(2):
-                pass_on(way, hop, j)
-                if hop == HOPS[way] - 1:
-                    packet_copy(way, 1, 2 + j).start()
-    select(LAST)
-    select(LAST - 1)
-    for hop in range(1, LAST - 1):
-        for j in range(2, 4):
-            for way in range(2):
-                pass_on(way, hop, j)
-        select(hop)
-        if hop == 2:
-            experts(LAST, LAST - 1)
-        if hop == LAST - 3:
-            send_back(LAST)
+    def meta_on(way, hop):
+        meta_copy(way, hop).wait_recv()
+        if hop < HOPS[way]:
+            meta_copy(way, hop + 1).start()
+
+    events = ring_order(prefix, T, [0.0] * (T // PIECE))
+    missing = {
+        hop: sum(-(-prefix(way, hop) // PIECE) for way in range(2)) for hop in range(1, LAST + 1)
+    }
+    deferred = []
+    begun = {(0, 0), (0, 1), (1, 0), (1, 1)}
+    seen = set()
+    for when, action, way, piece, hop in events:
+        while deferred and deferred[0][0] <= when:
+            deferred.pop(0)[1]()
+        if action == "own":
+            if (way, piece) not in begun:
+                packet_copy(way, 1, piece).start()
+            continue
+        if (way, hop) not in seen:
+            seen.add((way, hop))
+            meta_on(way, hop)
+        pass_on(way, hop, piece)
+        missing[hop] -= 1
+        if missing[hop] == 0:
+            select(hop)
+            if not missing[LAST] and not missing[LAST - 1] and not deferred and hop >= LAST - 1:
+                deferred = [
+                    (when + 12.0, lambda: experts(LAST, LAST - 1)),
+                    (when + 23.0, lambda: send_back(LAST)),
+                ]
+    for _, work in deferred:
+        work()
     send_back(LAST - 1)
     experts(LAST - 2, LAST - 3)
     experts(1, 2)
@@ -519,8 +577,8 @@
     for hop in range(LAST - 2, 0, -1):
         send_back(hop)
 
-    for j in range(T // CH):
-        rows = pl.ds(j * CH, CH)
+    for j in range(T // PIECE):
+        rows = pl.ds(j * PIECE, PIECE)
         for way in range(2):
             back_copy(way, 1, j).wait_recv()
         ret[0, 1, rows] = (ret[0, 1, rows].astype(F32) + acc[rows]).astype(BF)
@@ -535,8 +593,8 @@
     for way in range(2):
         for hop in range(1, HOPS[way] + 1):
             meta_copy(way, hop).wait_send()
-            for j in range(T // CH):
-                if j * CH < prefix(way, hop):
+            for j in range(T // PIECE):
+                if j * PIECE < prefix(way, hop):
                     packet_copy(way, hop, j).wait_send()
                     back_copy(way, hop, j).wait_send()
     for hop in range(1, LAST + 1):
@@ -580,7 +638,7 @@
         any_space = pl.BlockSpec(memory_space=pl.ANY)
         in_vmem = pl.BlockSpec(memory_space=pltpu.VMEM)
         dims = (T, D, Z, tp_count, sp_count, CAP, HEADS, HD)
-        chunks = T // (PL * CAP)
+        chunks = T // PIECE
         return pl.pallas_call(
             functools.partial(layer, dims),
             out_shape=jax.ShapeDtypeStruct((T, D), BF),

time: 205 us -> 210 us (1.024)
  Pallas kernels: 203 us -> 208 us
    pallas_call x1, Pallas kernels: 203 us -> 208 us  [on_device(): pl.pallas_call(functools.partial(layer, dims), out_shape=jax.ShapeDtypeSt...]
where the time goes in v3:
time: 210 us; the launch traced here: 209 us
  Pallas kernels  208 us (99%)
    pallas_call x1, Pallas kernels, on_device(): pl.pallas_call(functools.partial(layer, dims), out_shape=jax.ShapeDtypeSt...  208 us

profile of v3, /device:TPU:33, one launch (start us, length us, event | category | flops | bytes accessed | tf_op | source)
XLA Modules:
  0.0 209.4 jit_solution(8466961768773748725)
XLA Ops:
  0.0 207.5 %shard_map.118 = bf16[128,2048]{1,0:T(8,128)(2,1)} custom-call(bf16[512,512]{1,0:T(8,128)(2,1)} %q_hbm.1, bf16[64,512]{1,0:T(8,128)(2,1)} %bitcast.9, bf16[64,512]{1,0:T(8,128)(2,1)} %bitcast.10, f32[8]{0:T(128)} %sink_ref.1, bf16[512,2048]{1,0:T(8,128)(2,1)} %wo_hbm.1, bf16[128,2048]{1,0:T(8,128)(2,1)} %res_ref.1, f32[1,2048]{1,0:T(1,128)} %bitcast.11, ...), custom_call_target="tpu_custom_call" | custom-call | tf_op jit(solution)/shard_map/pallas_call | solution.py:642
  207.5 1.9 copy.14

commit v4 on v3

--- a/solution.py
+++ b/solution.py
@@ -84,12 +84,12 @@
     q_hbm,
     kt_hbm,
     vt_hbm,
-    sink_ref,
+    sink_hbm,
     wo_hbm,
-    res_ref,
-    gain_ref,
-    ids_ref,
-    rw_ref,
+    res_hbm,
+    gain_hbm,
+    ids_hbm,
+    rw_hbm,
     wg_hbm,
     wu_hbm,
     wd_hbm,
@@ -100,7 +100,13 @@
     wg,
     wu,
     wd,
+    sink_ref,
+    res_ref,
+    gain_ref,
+    ids_ref,
+    rw_ref,
     att,
+    att_c,
     s2,
     r2,
     sp,
@@ -115,6 +121,7 @@
     meta,
     table,
     place,
+    sorter,
     sel,
     xin,
     yout,
@@ -122,7 +129,10 @@
     ret,
     cbuf,
     load_sem,
+    kv_sem,
     halo_sem,
+    ids_send,
+    ids_recv,
     rs_send,
     rs_recv,
     d_send,
@@ -175,32 +185,45 @@
     s_after = {"sp": lax.rem(s + 1, SP), "tp": x}
     s_before = {"sp": lax.rem(s + SP - 1, SP), "tp": x}
 
-    loads = [
-        pltpu.make_async_copy(q_hbm, qv, load_sem.at[0]),
-        pltpu.make_async_copy(wo_hbm, wo, load_sem.at[1]),
-        pltpu.make_async_copy(wg_hbm.at[0], wg, load_sem.at[2]),
-        pltpu.make_async_copy(wu_hbm.at[0], wu, load_sem.at[3]),
-        pltpu.make_async_copy(wd_hbm.at[0], wd, load_sem.at[4]),
+    small = [
+        pltpu.make_async_copy(src, dst, load_sem.at[i])
+        for i, (src, dst) in enumerate(
+            (
+                (q_hbm, qv),
+                (sink_hbm, sink_ref),
+                (ids_hbm, ids_ref.at[0]),
+                (rw_hbm, rw_ref),
+            )
+        )
+    ]
+    wo_load = pltpu.make_async_copy(wo_hbm, wo, load_sem.at[4])
+    large = [
+        pltpu.make_async_copy(src, dst, load_sem.at[5 + i])
+        for i, (src, dst) in enumerate(
+            (
+                (res_hbm, res_ref),
+                (gain_hbm, gain_ref),
+                (wg_hbm.at[0], wg),
+                (wu_hbm.at[0], wu),
+                (wd_hbm.at[0], wd),
+            )
+        )
     ]
     kv_loads = []
     for b in range(TP):
         cols = pl.ds(b * T, T)
-        kv_loads.append(
-            pltpu.make_async_copy(kt_hbm.at[:, cols], kv.at[b + 1, pl.ds(0, HD)], load_sem.at[5 + b])
-        )
-        kv_loads.append(
-            pltpu.make_async_copy(
-                vt_hbm.at[:, cols], kv.at[b + 1, pl.ds(HD, HD)], load_sem.at[5 + TP + b]
+        for i, src in enumerate((kt_hbm, vt_hbm)):
+            kv_loads.append(
+                pltpu.make_async_copy(
+                    src.at[:, cols], kv.at[b + 1, pl.ds(i * HD, HD)], kv_sem.at[2 * b + i]
+                )
             )
-        )
     barrier = pltpu.get_barrier_semaphore()
     greeted = [ahead[0], ahead[1], s_after, s_before] + [peer(k) for k in range(1, PL)]
     for device in greeted:
         pl.semaphore_signal(barrier, inc=1, device_id=device, device_id_type=MESH)
-    for copy in kv_loads[::-1]:
+    for copy in kv_loads + small + [wo_load]:
         copy.start()
-    loads[0].start()
-    loads[1].start()
 
     halo = pltpu.make_async_remote_copy(
         src_ref=kv.at[TP],
@@ -230,7 +253,8 @@
             query = qv[rows, lanes]
             total = None
             for side in range(2):
-                sink = sink_ref[pair * 2 + side]
+                head = pair * 2 + side
+                sink = sink_ref[0:1, head : head + 1]
                 score = mm(query, keys[side]) * (HD ** (-0.5))
                 score = jnp.where(allowed, score, -jnp.inf)
                 top = jnp.maximum(jnp.max(score, axis=1, keepdims=True), sink)
@@ -240,100 +264,151 @@
                 total = mixed if total is None else total + mixed
             att[slot, :, lanes] = total.astype(BF)
 
-    def rs_copy(src, dst, index, device):
-        return pltpu.make_async_remote_copy(
-            src_ref=src,
-            dst_ref=dst,
-            send_sem=rs_send.at[index],
-            recv_sem=rs_recv.at[index],
-            device_id=device,
-            device_id_type=MESH,
-        )
-
-    def project(slot, half):
-        return mm(att[slot], wo[:, pl.ds(half * HALF, HALF)])
-
-    right, left = to_x(1), to_x(-1)
-    for copy in kv_loads:
-        copy.wait()
-    loads[0].wait()
-    attend(1, 1)
-    pl.semaphore_wait(barrier, len(greeted))
-    halo.start()
-    for copy in loads[2:]:
-        copy.start()
-    for b in range(2, TP):
-        attend(b, b)
-    loads[1].wait()
-    halo.wait()
-    attend(0, 0)
-    far, after, prior = lax.rem(x + 2, TP), lax.rem(x + 1, TP), lax.rem(x + TP - 1, TP)
-    copies = []
-    for half, device in ((0, right), (1, left)):
-        s2[half] = project(far, half).astype(BF)
-        copy = rs_copy(s2.at[half], r2.at[half], half, device)
-        copy.start()
-        copies.append(copy)
-    sp[1] = project(after, 1).astype(BF)
-    send_p1 = rs_copy(sp.at[1], rp.at[1], 2, right)
-    send_p1.start()
-    sm[0] = project(prior, 0).astype(BF)
-    send_m0 = rs_copy(sm.at[0], rm.at[0], 3, left)
-    send_m0.start()
-    for half in range(2):
-        cols = pl.ds(half * HALF, HALF)
-        acc[:, cols] = project(x, half) + res_ref[:, cols].astype(F32)
-    early = project(after, 0)
-    copies[0].wait_recv()
-    sp[0] = (early + r2[0].astype(F32)).astype(BF)
-    send_p0 = rs_copy(sp.at[0], rp.at[0], 4, right)
-    send_p0.start()
-    early = project(prior, 1)
-    copies[1].wait_recv()
-    sm[1] = (early + r2[1].astype(F32)).astype(BF)
-    send_m1 = rs_copy(sm.at[1], rm.at[1], 5, left)
-    send_m1.start()
-
     E = Z * PL
+    plane_bits = PL.bit_length() - 1
     e_sub = iota((E, T), 0)
-    t_lane = iota((E, T), 1)
-    first_id = ids_ref[0:1, :]
-    second_id = ids_ref[1:2, :]
-    took0 = jnp.where(e_sub == first_id, 1.0, 0.0).astype(F32)
-    took1 = jnp.where(e_sub == second_id, 1.0, 0.0).astype(F32)
-    took = took0 + took1
-    before = jnp.where(iota((T, T), 0) < iota((T, T), 1), 1.0, 0.0).astype(BF)
-    rank = mm(took.astype(BF), before)
-    weight_a = rw_ref[0:1, :]
-    weight_b = rw_ref[1:2, :]
-    whole = weight_a + weight_b
-    share = took0 * (weight_a / whole) + took1 * (weight_b / whole)
-    plane_bits = PL.bit_length() - 1
-    e_plane = lax.shift_right_logical(e_sub, plane_bits)
-    rel = (e_plane - z) * (1 - 2 * c) + 2 * Z
+    t_sub = iota((T, T), 0)
+    t_col = iota((T, T), 1)
+    rel = (lax.shift_right_logical(e_sub, plane_bits) - z) * (1 - 2 * c) + 2 * Z
     rel = rel & (Z - 1)
     is_a = (rel >= 1) & (rel <= HOPS[0])
     dist = (
         jnp.where(is_a, rel, 0).astype(F32),
         jnp.where(rel > HOPS[0], Z - rel, 0).astype(F32),
     )
-    t_sub = iota((T, T), 0)
-    t_col = iota((T, T), 1)
-    positions = []
-    for way in range(2):
-        far = jnp.max(took * dist[way], axis=0, keepdims=True)
-        along = jnp.broadcast_to(far, (T, T))
+
+    def rank_of(key):
+        along = jnp.broadcast_to(key, (T, T))
         down = along.T
         ahead_of = (down > along) | ((down == along) & (t_sub < t_col))
-        positions.append(jnp.sum(jnp.where(ahead_of, 1.0, 0.0), axis=0, keepdims=True))
-    for way in range(2):
-        place[way] = jnp.where(positions[way] == t_sub.astype(F32), 1.0, 0.0).astype(BF)
+        return jnp.sum(jnp.where(ahead_of, 1.0, 0.0), axis=0, keepdims=True)
+
+    def orders(slot):
+        took = [
+            jnp.where(e_sub == ids_ref[slot, k : k + 1, :], 1.0, 0.0).astype(F32) for k in range(2)
+        ]
+        both = took[0] + took[1]
+        ways = [rank_of(jnp.max(both * d, axis=0, keepdims=True)) for d in dist]
+        return took, ways, rank_of(-jnp.minimum(ways[0], ways[1]))
+
+    def placing(position):
+        return jnp.where(position == t_sub.astype(F32), 1.0, 0.0).astype(BF)
+
+    right, left = to_x(1), to_x(-1)
+    QUARTERS = T // CH
+
+    def rs_copy(kind, q):
+        src, dst, half, device, group = (
+            (s2, r2, 0, right, 0),
+            (s2, r2, 1, left, 0),
+            (sp, rp, 1, right, 1),
+            (sm, rm, 0, left, 2),
+            (sp, rp, 0, right, 1),
+            (sm, rm, 1, left, 2),
+        )[kind]
+        rows = pl.ds(q * CH, CH)
+        return pltpu.make_async_remote_copy(
+            src_ref=src.at[half, rows],
+            dst_ref=dst.at[half, rows],
+            send_sem=rs_send.at[group],
+            recv_sem=rs_recv.at[kind * QUARTERS + q],
+            device_id=device,
+            device_id_type=MESH,
+        )
+
+    def first_leg(q):
+        rs_copy(0, q).start()
+        rs_copy(1, q).start()
+
+    def alone(q):
+        rs_copy(2, q).start()
+        rs_copy(3, q).start()
+
+    def joined(q):
+        rows = pl.ds(q * CH, CH)
+        for kind, dst, half in ((0, sp, 0), (1, sm, 1)):
+            rs_copy(kind, q).wait_recv()
+            total = cbuf[half, rows, pl.ds(0, HALF)] + r2[half, rows].astype(F32)
+            dst[half, rows] = total.astype(BF)
+            rs_copy(4 + kind, q).start()
+
+    def project(slot, half):
+        return mm(att_c[slot], wo[:, pl.ds(half * HALF, HALF)])
+
+    def ids_copy(m):
+        return pltpu.make_async_remote_copy(
+            src_ref=ids_ref.at[0],
+            dst_ref=ids_ref.at[m],
+            send_sem=ids_send.at[m],
+            recv_sem=ids_recv.at[m],
+            device_id=to_x(-m),
+            device_id_type=MESH,
+        )
+
+    for copy in kv_loads + small:
+        copy.wait()
+    attend(1, 1)
+    pl.semaphore_wait(barrier, len(greeted))
+    halo.start()
+    for m in range(1, TP):
+        ids_copy(m).start()
+    for copy in large:
+        copy.start()
+    for b in range(2, TP):
+        attend(b, b)
+    took, positions, position_c = orders(0)
+    place[0] = placing(positions[0])
+    place[1] = placing(positions[1])
+    place[2] = placing(position_c)
+    halo.wait_recv()
+    attend(0, 0)
+    for m in range(1, TP):
+        ids_copy(m).wait_recv()
+
+    def arrange(m, placed):
+        att_c[m] = mm(placed, att[lax.rem(x + m, TP)]).astype(BF)
+
+    far, after, prior = 2, 1, TP - 1
+    arrange(far, placing(orders(far)[2]))
+    wo_load.wait()
+    for half in range(2):
+        s2[half] = project(far, half).astype(BF)
+    first_leg(0)
+    for m in (after, prior):
+        arrange(m, placing(orders(m)[2]))
+    sp[1] = project(after, 1).astype(BF)
+    sm[0] = project(prior, 0).astype(BF)
+    alone(0)
+    first_leg(1)
+    first_leg(2)
+    cbuf[0, :, pl.ds(0, HALF)] = project(after, 0)
+    cbuf[1, :, pl.ds(0, HALF)] = project(prior, 1)
+    joined(0)
+    alone(1)
+    first_leg(3)
+    large[0].wait()
+    large[1].wait()
+    arrange(0, place[2])
+    for half in range(2):
+        cols = pl.ds(half * HALF, HALF)
+        acc[:, cols] = project(0, half) + mm(place[2], res_ref[:, cols])
+    joined(1)
+    alone(2)
+
+    t_lane = iota((E, T), 1)
+    either = took[0] + took[1]
+    before = jnp.where(t_sub < t_col, 1.0, 0.0).astype(BF)
+    rank = mm(either.astype(BF), before)
+    weight_a = rw_ref[0:1, :]
+    weight_b = rw_ref[1:2, :]
+    whole = weight_a + weight_b
+    share = took[0] * (weight_a / whole) + took[1] * (weight_b / whole)
     slot_value = jnp.where(is_a, positions[0] + 1.0, positions[1] + (1.0 + T))
     base = (e_sub & (PL - 1)) * GR + jnp.where(is_a, 0, CAP)
     spread_t = jnp.zeros((E, T), F32)
     spread_w = jnp.zeros((E, T), F32)
     for r in range(CAP):
-        here = took * jnp.where(rank == float(r), 1.0, 0.0)
+        here = either * jnp.where(rank == float(r), 1.0, 0.0)
         value_col = jnp.sum(here * slot_value, axis=1, keepdims=True)
         share_col = jnp.sum(here * share, axis=1, keepdims=True)
         hit = t_lane == base + r
@@ -345,6 +420,9 @@
     OWN = HOPS[0] - 1
     meta[OWN, 1, pl.ds(0, Z)] = mm(plane_of, spread_t.astype(BF)).astype(BF)
     meta[OWN, 1, pl.ds(Z, Z)] = mm(plane_of, spread_w.astype(BF)).astype(BF)
+    for way in range(2):
+        sorter[way] = mm_nt(place[way], place[2]).astype(BF)
+    normed[...] = jnp.zeros((T, D), BF)
 
     prefix = prefix_rows(HOPS, T, CH)
     for way in range(2):
@@ -352,15 +430,14 @@
             n = prefix(way, hop)
             if n < T:
                 ring[hop - 1, way, pl.ds(n, T - n)] = jnp.zeros((T - n, D), BF)
-
-    send_p1.wait_recv()
-    send_p0.wait_recv()
-    send_m0.wait_recv()
-    send_m1.wait_recv()
-    ROWS = 32
-    for r in range(T // ROWS):
-        rows = pl.ds(r * ROWS, ROWS)
-        square = jnp.zeros((ROWS, 1), F32)
+    joined(2)
+    alone(3)
+
+    def prepare(q):
+        for kind in range(2, 6):
+            rs_copy(kind, q).wait_recv()
+        rows = pl.ds(q * CH, CH)
+        square = jnp.zeros((CH, 1), F32)
         for half in range(2):
             cols = pl.ds(half * HALF, HALF)
             total = acc[rows, cols] + rp[half, rows].astype(F32) + rm[half, rows].astype(F32)
@@ -373,9 +450,22 @@
             cols = pl.ds(half * HALF, HALF)
             wide = stream[rows, cols].astype(F32)
             normed[rows, cols] = (wide * scale * gain_ref[:, cols]).astype(BF)
+        count = PIECE if q < QUARTERS - 1 else T - q * PIECE
+        rows = pl.ds(q * PIECE, count)
+        own_a[rows] = mm(sorter[0, rows], normed[...]).astype(BF)
+        ring[OWN, 1, rows] = mm(sorter[1, rows], normed[...]).astype(BF)
+
+    first_index, pieces = {}, 0
+    for way in range(2):
+        for hop in range(1, HOPS[way] + 1):
+            first_index[way, hop] = pieces
+            pieces += prefix(way, hop) // PIECE
 
     def d_index(way, hop, j):
-        return (way * HOPS[0] + hop - 1) * (T // PIECE) + j
+        return first_index[way, hop] + j
+
+    def hop_index(way, hop):
+        return way * HOPS[0] + hop - 1
 
     def packet_copy(way, hop, j):
         rows = pl.ds(j * PIECE, PIECE)
@@ -387,7 +477,7 @@
         return pltpu.make_async_remote_copy(
             src_ref=src,
             dst_ref=ring.at[hop - 1, way, rows],
-            send_sem=d_send.at[index],
+            send_sem=d_send.at[hop_index(way, hop)],
             recv_sem=d_recv.at[index],
             device_id=ahead[way],
             device_id_type=MESH,
@@ -395,7 +485,7 @@
 
     def meta_copy(way, hop):
         src = meta.at[OWN, 1] if hop == 1 else meta.at[hop - 2, way]
-        index = way * HOPS[0] + hop - 1
+        index = hop_index(way, hop)
         return pltpu.make_async_remote_copy(
             src_ref=src,
             dst_ref=meta.at[hop - 1, way],
@@ -407,14 +497,10 @@
 
     for way in range(2):
         meta_copy(way, 1).start()
-    for j in range(T // CH):
-        rows = pl.ds(j * CH, CH)
-        own_a[rows] = mm(place[0, rows], normed[...]).astype(BF)
-        ring[OWN, 1, rows] = mm(place[1, rows], normed[...]).astype(BF)
-        if j == 0:
-            for way in range(2):
-                for i in range(2):
-                    packet_copy(way, 1, i).start()
+    prepare(0)
+    for way in range(2):
+        packet_copy(way, 1, 0).start()
+    joined(QUARTERS - 1)
 
     def hop_table(hop):
         picked_t = jnp.zeros((1, T), F32)
@@ -428,26 +514,25 @@
         table[hop - 1, 1:2] = picked_w
 
     def plane_copy(buffer_from, buffer_to, sends, recvs, hop, k):
-        index = (hop - 1) * PL + k
         return pltpu.make_async_remote_copy(
             src_ref=buffer_from.at[hop - 1, peer_rank(k)],
             dst_ref=buffer_to.at[hop - 1, me],
-            send_sem=sends.at[index],
-            recv_sem=recvs.at[index],
+            send_sem=sends.at[hop - 1],
+            recv_sem=recvs.at[hop - 1],
             device_id=peer(k),
             device_id_type=MESH,
         )
 
-    def plane_wait(buffer_from, buffer_to, sends, recvs, hop, k):
-        index = (hop - 1) * PL + k
-        pltpu.make_async_remote_copy(
-            src_ref=buffer_from.at[hop - 1, from_rank(k)],
-            dst_ref=buffer_to.at[hop - 1, from_rank(k)],
-            send_sem=sends.at[index],
-            recv_sem=recvs.at[index],
-            device_id=peer(k),
+    def plane_all(buffer_from, buffer_to, sends, recvs, hop):
+        blocks = pl.ds(0, PL - 1)
+        return pltpu.make_async_remote_copy(
+            src_ref=buffer_from.at[hop - 1, blocks],
+            dst_ref=buffer_to.at[hop - 1, blocks],
+            send_sem=sends.at[hop - 1],
+            recv_sem=recvs.at[hop - 1],
+            device_id=peer(1),
             device_id_type=MESH,
-        ).wait_recv()
+        )
 
     COLS = 512
 
@@ -465,8 +550,7 @@
 
     def experts(*hops):
         for hop in hops:
-            for k in range(1, PL):
-                plane_wait(sel, xin, p_send, p_recv, hop, k)
+            plane_all(sel, xin, p_send, p_recv, hop).wait_recv()
         rows = jnp.concatenate(
             [xin[hop - 1].astype(F32).reshape(SEL, D).astype(BF) for hop in hops], axis=0
         )
@@ -490,15 +574,14 @@
         return pltpu.make_async_remote_copy(
             src_ref=ret.at[hop, way, rows],
             dst_ref=ret.at[hop - 1, way, rows],
-            send_sem=b_send.at[index],
+            send_sem=b_send.at[hop_index(way, hop)],
             recv_sem=b_recv.at[index],
             device_id=behind[way],
             device_id_type=MESH,
         )
 
     def weighted(hop, ways):
-        for k in range(1, PL):
-            plane_wait(yout, zin, y_send, y_recv, hop, k)
+        plane_all(yout, zin, y_send, y_recv, hop).wait_recv()
         mixes = []
         for way, n in ways:
             spot = (iota((n, SEL), 0) + (way * T + 1)).astype(F32)
@@ -535,25 +618,29 @@
         if j * PIECE < prefix(way, hop + 1):
             packet_copy(way, hop + 1, j).start()
 
-    for copy in loads[2:]:
+    for copy in large[2:]:
         copy.wait()
     def meta_on(way, hop):
         meta_copy(way, hop).wait_recv()
         if hop < HOPS[way]:
             meta_copy(way, hop + 1).start()
 
-    events = ring_order(prefix, T, [0.0] * (T // PIECE))
+    ready = [0.0, 6.0, 10.0] + [14.0] * (T // PIECE - QUARTERS + 1)
+    events = ring_order(prefix, T, ready)
+    prepared = 1
     missing = {
         hop: sum(-(-prefix(way, hop) // PIECE) for way in range(2)) for hop in range(1, LAST + 1)
     }
     deferred = []
-    begun = {(0, 0), (0, 1), (1, 0), (1, 1)}
     seen = set()
     for when, action, way, piece, hop in events:
         while deferred and deferred[0][0] <= when:
             deferred.pop(0)[1]()
         if action == "own":
-            if (way, piece) not in begun:
+            if prepared < QUARTERS and piece >= prepared:
+                prepare(prepared)
+                prepared += 1
+            if piece > 0:
                 packet_copy(way, 1, piece).start()
             continue
         if (way, hop) not in seen:
@@ -564,12 +651,10 @@
         if missing[hop] == 0:
             select(hop)
             if not missing[LAST] and not missing[LAST - 1] and not deferred and hop >= LAST - 1:
-                deferred = [
-                    (when + 12.0, lambda: experts(LAST, LAST - 1)),
-                    (when + 23.0, lambda: send_back(LAST)),
-                ]
+                deferred = [(when + 12.0, lambda: experts(LAST, LAST - 1))]
     for _, work in deferred:
         work()
+    send_back(LAST)
     send_back(LAST - 1)
     experts(LAST - 2, LAST - 3)
     experts(1, 2)
@@ -582,25 +667,40 @@
         for way in range(2):
             back_copy(way, 1, j).wait_recv()
         ret[0, 1, rows] = (ret[0, 1, rows].astype(F32) + acc[rows]).astype(BF)
-    unsort = place[...].reshape(2 * T, T)
+    unsort = place[pl.ds(0, 2)].reshape(2 * T, T)
     for n in range(D // COLS):
         cols = pl.ds(n * COLS, COLS)
         came = ret[0, :, :, cols].reshape(2 * T, COLS)
-        out_ref[:, cols] = (stream[:, cols].astype(F32) + mm_tn(unsort, came)).astype(BF)
-
-    for copy in copies + [send_p1, send_m0, send_p0, send_m1]:
-        copy.wait_send()
+        out_ref[:, cols] = (mm_tn(place[2], stream[:, cols]) + mm_tn(unsort, came)).astype(BF)
+
+    halo.wait_send()
+    for m in range(1, TP):
+        ids_copy(m).wait_send()
+    for group, (src, dst) in enumerate(((s2, r2), (sp, rp), (sm, rm))):
+        pltpu.make_async_remote_copy(
+            src_ref=src,
+            dst_ref=dst,
+            send_sem=rs_send.at[group],
+            recv_sem=rs_recv.at[0],
+            device_id=right,
+            device_id_type=MESH,
+        ).wait_send()
     for way in range(2):
         for hop in range(1, HOPS[way] + 1):
             meta_copy(way, hop).wait_send()
-            for j in range(T // PIECE):
-                if j * PIECE < prefix(way, hop):
-                    packet_copy(way, hop, j).wait_send()
-                    back_copy(way, hop, j).wait_send()
+            rows = pl.ds(0, prefix(way, hop))
+            for buffer, sems, recvs in ((ring, d_send, d_recv), (ret, b_send, b_recv)):
+                pltpu.make_async_remote_copy(
+                    src_ref=buffer.at[hop - 1, way, rows],
+                    dst_ref=buffer.at[hop - 1, way, rows],
+                    send_sem=sems.at[hop_index(way, hop)],
+                    recv_sem=recvs.at[0],
+                    device_id=ahead[way],
+                    device_id_type=MESH,
+                ).wait_send()
     for hop in range(1, LAST + 1):
-        for k in range(1, PL):
-            plane_copy(sel, xin, p_send, p_recv, hop, k).wait_send()
-            plane_copy(yout, zin, y_send, y_recv, hop, k).wait_send()
+        plane_all(sel, xin, p_send, p_recv, hop).wait_send()
+        plane_all(yout, zin, y_send, y_recv, hop).wait_send()
 
 
 def solution(mesh):
@@ -638,24 +738,13 @@
         any_space = pl.BlockSpec(memory_space=pl.ANY)
         in_vmem = pl.BlockSpec(memory_space=pltpu.VMEM)
         dims = (T, D, Z, tp_count, sp_count, CAP, HEADS, HD)
-        chunks = T // PIECE
+        quarters = T // (PL * CAP)
+        prefix = prefix_rows((HOP, HOP - 1), T, PL * CAP)
+        pieces = sum(prefix(way, hop) // PIECE for way in range(2) for hop in range(1, HOP + 1))
         return pl.pallas_call(
             functools.partial(layer, dims),
             out_shape=jax.ShapeDtypeStruct((T, D), BF),
-            in_specs=[
-                any_space,
-                any_space,
-                any_space,
-                pl.BlockSpec(memory_space=pltpu.SMEM),
-                any_space,
-                in_vmem,
-                in_vmem,
-                in_vmem,
-                in_vmem,
-                any_space,
-                any_space,
-                any_space,
-            ],
+            in_specs=[any_space] * 12,
             out_specs=in_vmem,
             scratch_shapes=[
                 vm(queries.shape, BF),
@@ -664,7 +753,13 @@
                 vm((D, FF), BF),
                 vm((D, FF), BF),
                 vm((FF, D), BF),
-                vm((4, T, HEADS * HD), BF),
+                vm((1, HEADS), F32),
+                vm((T, D), BF),
+                vm((1, D), F32),
+                vm((tp_count, top_k, T), jnp.int32),
+                vm((top_k, T), F32),
+                vm((tp_count, T, HEADS * HD), BF),
+                vm((tp_count, T, HEADS * HD), BF),
                 vm((2, T, D // 2), BF),
                 vm((2, T, D // 2), BF),
                 vm((2, T, D // 2), BF),
@@ -678,6 +773,7 @@
                 vm((HOP, 2, T, D), BF),
                 vm((HOP, 2, 2 * Z, T), BF),
                 vm((HOP, 8, T), F32),
+                vm((3, T, T), BF),
                 vm((2, T, T), BF),
                 vm((HOP, PL, GR, D), BF),
                 vm((HOP, PL, GR, D), BF),
@@ -685,20 +781,23 @@
                 vm((HOP, PL, GR, D), BF),
                 vm((HOP + 1, 2, T, D), BF),
                 vm((2, T, D), F32),
-                dma((5 + 2 * tp_count,)),
+                dma((10,)),
+                dma((2 * tp_count,)),
                 dma((2,)),
-                dma((6,)),
-                dma((6,)),
-                dma((2 * HOP * chunks,)),
-                dma((2 * HOP * chunks,)),
+                dma((tp_count,)),
+                dma((tp_count,)),
+                dma((3,)),
+                dma((6 * quarters,)),
+                dma((2 * HOP,)),
+                dma((pieces,)),
                 dma((2 * HOP,)),
                 dma((2 * HOP,)),
-                dma((HOP * PL,)),
-                dma((HOP * PL,)),
-                dma((HOP * PL,)),
-                dma((HOP * PL,)),
-                dma((2 * HOP * chunks,)),
-                dma((2 * HOP * chunks,)),
+                dma((HOP,)),
+                dma((HOP,)),
+                dma((HOP,)),
+                dma((HOP,)),
+                dma((2 * HOP,)),
+                dma((pieces,)),
             ],
             compiler_params=pltpu.CompilerParams(
                 collective_id=0, has_side_effects=True, vmem_limit_bytes=62 * 1024 * 1024
@@ -707,7 +806,7 @@
             queries,
             keys_t,
             values_t,
-            sink_logit,
+            sink_logit.reshape(1, HEADS),
             out_weight,
             residual,
             norm_gain.reshape(1, D),

time: 210 us -> 204 us (0.971)
  Pallas kernels: 208 us -> 202 us
    pallas_call x1, Pallas kernels: 208 us -> 202 us  [on_device(): pl.pallas_call(functools.partial(layer, dims), out_shape=jax.ShapeDtypeSt...]
where the time goes in v4:
time: 204 us
  Pallas kernels  202 us (99%)
    pallas_call x1, Pallas kernels, on_device(): pl.pallas_call(functools.partial(layer, dims), out_shape=jax.ShapeDtypeSt...  202 us

profile of v4, /device:TPU:33, one launch (start us, length us, event | category | flops | bytes accessed | tf_op | source)
XLA Modules:
  0.0 204.2 jit_solution(10929486038028318033)
XLA Ops:
  0.0 202.4 %shard_map.118 = bf16[128,2048]{1,0:T(8,128)(2,1)} custom-call(bf16[512,512]{1,0:T(8,128)(2,1)} %q_hbm.1, bf16[64,512]{1,0:T(8,128)(2,1)} %bitcast.10, bf16[64,512]{1,0:T(8,128)(2,1)} %bitcast.11, f32[1,8]{1,0:T(1,128)} %bitcast.15, bf16[512,2048]{1,0:T(8,128)(2,1)} %wo_hbm.1, bf16[128,2048]{1,0:T(8,128)(2,1)} %res_hbm.1, f32[1,2048]{1,0:T(1,128)} %bitcast.12, ...), custom_call_target="tpu_custom_call" | custom-call | tf_op jit(solution)/shard_map/pallas_call | solution.py:744
  202.4 1.9 copy.14

commit v5 on v4

--- a/solution.py
+++ b/solution.py
@@ -41,16 +41,16 @@
     return prefix
 
 
-def ring_order(prefix, rows, ready, latency=3.0, waiting=1):
+def ring_order(prefix, order, ready, waiting, latency=3.0):
     queue, left, now, clock = ([], []), [0.0, 0.0], [None, None], 0.0
-    own = [list(range(rows // PIECE)) for _ in range(2)]
+    own = [list(order), list(order)]
     coming, events = [], []
     while True:
         for way in range(2):
             while (
                 own[way]
                 and ready[own[way][0]] <= clock + 1e-6
-                and len(queue[way]) + (now[way] is not None) <= waiting
+                and len(queue[way]) + (now[way] is not None) <= waiting[own[way][0]]
             ):
                 piece = own[way].pop(0)
                 queue[way].append((piece, 1))
@@ -254,7 +254,7 @@
             total = None
             for side in range(2):
                 head = pair * 2 + side
-                sink = sink_ref[0:1, head : head + 1]
+                sink = sink_ref[0, head]
                 score = mm(query, keys[side]) * (HD ** (-0.5))
                 score = jnp.where(allowed, score, -jnp.inf)
                 top = jnp.maximum(jnp.max(score, axis=1, keepdims=True), sink)
@@ -373,7 +373,7 @@
     wo_load.wait()
     for half in range(2):
         s2[half] = project(far, half).astype(BF)
-    first_leg(0)
+        rs_copy(half, 0).start()
     for m in (after, prior):
         arrange(m, placing(orders(m)[2]))
     sp[1] = project(after, 1).astype(BF)
@@ -625,19 +625,21 @@
         if hop < HOPS[way]:
             meta_copy(way, hop + 1).start()
 
-    ready = [0.0, 6.0, 10.0] + [14.0] * (T // PIECE - QUARTERS + 1)
-    events = ring_order(prefix, T, ready)
+    last_quarter = T // PIECE - QUARTERS + 1
+    ready = [0.0, 5.8, 9.6] + [13.5] * last_quarter
+    events = ring_order(prefix, (0, 1, 2, 4, 5, 3, 6, 7), ready, (3, 3, 3, 3, 3, 3, 2, 2))
     prepared = 1
     missing = {
-        hop: sum(-(-prefix(way, hop) // PIECE) for way in range(2)) for hop in range(1, LAST + 1)
+        hop: sum(prefix(way, hop) // PIECE for way in range(2)) for hop in range(1, LAST + 1)
     }
-    deferred = []
+    groups = [(LAST, LAST - 1), (LAST - 2,)]
+    later = []
     seen = set()
     for when, action, way, piece, hop in events:
-        while deferred and deferred[0][0] <= when:
-            deferred.pop(0)[1]()
+        while later and later[0][0] <= when:
+            experts(*later.pop(0)[1])
         if action == "own":
-            if prepared < QUARTERS and piece >= prepared:
+            while prepared <= min(piece, QUARTERS - 1):
                 prepare(prepared)
                 prepared += 1
             if piece > 0:
@@ -650,16 +652,18 @@
         missing[hop] -= 1
         if missing[hop] == 0:
             select(hop)
-            if not missing[LAST] and not missing[LAST - 1] and not deferred and hop >= LAST - 1:
-                deferred = [(when + 12.0, lambda: experts(LAST, LAST - 1))]
-    for _, work in deferred:
-        work()
+            for group in groups:
+                if hop in group and not any(missing[h] for h in group):
+                    later.append((when + 12.0, group))
+    for _, group in later:
+        experts(*group)
     send_back(LAST)
     send_back(LAST - 1)
-    experts(LAST - 2, LAST - 3)
+    experts(LAST - 3)
+    send_back(LAST - 2)
     experts(1, 2)
     experts(3, 4)
-    for hop in range(LAST - 2, 0, -1):
+    for hop in range(LAST - 3, 0, -1):
         send_back(hop)
 
     for j in range(T // PIECE):
@@ -753,7 +757,7 @@
                 vm((D, FF), BF),
                 vm((D, FF), BF),
                 vm((FF, D), BF),
-                vm((1, HEADS), F32),
+                pltpu.SMEM((1, HEADS), F32),
                 vm((T, D), BF),
                 vm((1, D), F32),
                 vm((tp_count, top_k, T), jnp.int32),

time: 204 us -> 204 us (level)
  no operation moved by 1% of the time
where the time goes in v5:
time: 204 us
  Pallas kernels  202 us (99%)
    pallas_call x1, Pallas kernels, on_device(): pl.pallas_call(functools.partial(layer, dims), out_shape=jax.ShapeDtypeSt...  202 us

profile of v5, /device:TPU:33, one launch (start us, length us, event | category | flops | bytes accessed | tf_op | source)
XLA Modules:
  0.0 203.8 jit_solution(6363905258297389870)
XLA Ops:
  0.0 201.9 %shard_map.118 = bf16[128,2048]{1,0:T(8,128)(2,1)} custom-call(bf16[512,512]{1,0:T(8,128)(2,1)} %q_hbm.1, bf16[64,512]{1,0:T(8,128)(2,1)} %bitcast.10, bf16[64,512]{1,0:T(8,128)(2,1)} %bitcast.11, f32[1,8]{1,0:T(1,128)} %bitcast.15, bf16[512,2048]{1,0:T(8,128)(2,1)} %wo_hbm.1, bf16[128,2048]{1,0:T(8,128)(2,1)} %res_hbm.1, f32[1,2048]{1,0:T(1,128)} %bitcast.12, ...), custom_call_target="tpu_custom_call" | custom-call | tf_op jit(solution)/shard_map/pallas_call | solution.py:748
  201.9 1.9 copy.14

commit v6 on v5

--- a/solution.py
+++ b/solution.py
@@ -32,6 +32,13 @@
 
 
 PIECE = 16
+ORDER = (0, 1, 2, 3, 4, 5, 6, 7)
+WAITING = (1, 1, 1, 1, 1, 1, 1, 1)
+READY = (0.0, 5.8, 9.6, 13.5)
+LATENCY = 3.9
+EARLY = ((8, 7),)
+TAIL = 0
+PEERS = (1, 2, 3, 4, 5, 6, 7)
 
 
 def prefix_rows(hops, rows, share):
@@ -544,7 +551,7 @@
             cols = pl.ds(n * COLS, COLS)
             rows = ring[hop - 1, :, :, cols].reshape(2 * T, COLS)
             sel[hop - 1, :, :, cols] = mm_tn(hot, rows).reshape(PL, GR, COLS).astype(BF)
-        for k in range(1, PL):
+        for k in PEERS:
             plane_copy(sel, xin, p_send, p_recv, hop, k).start()
         xin[hop - 1, me] = sel[hop - 1, me]
 
@@ -564,7 +571,7 @@
                 part = product[i * SEL : (i + 1) * SEL]
                 yout[hop - 1, :, :, cols] = part.reshape(PL, GR, COLS).astype(BF)
         for hop in hops:
-            for k in range(1, PL):
+            for k in PEERS:
                 plane_copy(yout, zin, y_send, y_recv, hop, k).start()
             zin[hop - 1, me] = yout[hop - 1, me]
 
@@ -625,14 +632,12 @@
         if hop < HOPS[way]:
             meta_copy(way, hop + 1).start()
 
-    last_quarter = T // PIECE - QUARTERS + 1
-    ready = [0.0, 5.8, 9.6] + [13.5] * last_quarter
-    events = ring_order(prefix, (0, 1, 2, 4, 5, 3, 6, 7), ready, (3, 3, 3, 3, 3, 3, 2, 2))
+    ready = list(READY) + [READY[-1]] * (T // PIECE - QUARTERS)
+    events = ring_order(prefix, ORDER, ready, WAITING, LATENCY)
     prepared = 1
     missing = {
         hop: sum(prefix(way, hop) // PIECE for way in range(2)) for hop in range(1, LAST + 1)
     }
-    groups = [(LAST, LAST - 1), (LAST - 2,)]
     later = []
     seen = set()
     for when, action, way, piece, hop in events:
@@ -652,18 +657,45 @@
         missing[hop] -= 1
         if missing[hop] == 0:
             select(hop)
-            for group in groups:
+            for group in EARLY:
                 if hop in group and not any(missing[h] for h in group):
                     later.append((when + 12.0, group))
     for _, group in later:
         experts(*group)
-    send_back(LAST)
-    send_back(LAST - 1)
-    experts(LAST - 3)
-    send_back(LAST - 2)
-    experts(1, 2)
-    experts(3, 4)
-    for hop in range(LAST - 3, 0, -1):
+    if TAIL == 0:
+        send_back(8)
+        send_back(7)
+        experts(6, 5)
+        experts(1, 2)
+        experts(3, 4)
+        rest = range(6, 0, -1)
+    elif TAIL == 1:
+        send_back(8)
+        send_back(7)
+        experts(6)
+        experts(5)
+        send_back(6)
+        experts(1, 2)
+        experts(3, 4)
+        rest = range(5, 0, -1)
+    elif TAIL == 2:
+        send_back(8)
+        experts(5)
+        send_back(7)
+        experts(6)
+        experts(3, 4)
+        send_back(6)
+        experts(1, 2)
+        rest = range(5, 0, -1)
+    elif TAIL == 3:
+        send_back(8)
+        send_back(7)
+        experts(5)
+        send_back(6)
+        experts(1, 2)
+        experts(3, 4)
+        rest = range(5, 0, -1)
+    for hop in rest:
         send_back(hop)
 
     for j in range(T // PIECE):

time: 204 us -> 197 us (0.966)
  Pallas kernels: 202 us -> 195 us
    pallas_call x1, Pallas kernels: 202 us -> 195 us  [on_device(): pl.pallas_call(functools.partial(layer, dims), out_shape=jax.ShapeDtypeSt...]
where the time goes in v6:
time: 197 us
  Pallas kernels  195 us (99%)
    pallas_call x1, Pallas kernels, on_device(): pl.pallas_call(functools.partial(layer, dims), out_shape=jax.ShapeDtypeSt...  195 us

profile of v6, /device:TPU:33, one launch (start us, length us, event | category | flops | bytes accessed | tf_op | source)
XLA Modules:
  0.0 196.9 jit_solution(4898508264109076721)
XLA Ops:
  0.0 195.0 %shard_map.118 = bf16[128,2048]{1,0:T(8,128)(2,1)} custom-call(bf16[512,512]{1,0:T(8,128)(2,1)} %q_hbm.1, bf16[64,512]{1,0:T(8,128)(2,1)} %bitcast.10, bf16[64,512]{1,0:T(8,128)(2,1)} %bitcast.11, f32[1,8]{1,0:T(1,128)} %bitcast.15, bf16[512,2048]{1,0:T(8,128)(2,1)} %wo_hbm.1, bf16[128,2048]{1,0:T(8,128)(2,1)} %res_hbm.1, f32[1,2048]{1,0:T(1,128)} %bitcast.12, ...), custom_call_target="tpu_custom_call" | custom-call | tf_op jit(solution)/shard_map/pallas_call | solution.py:780
  195.0 1.9 copy.14

commit v7 on v6

--- a/solution.py
+++ b/solution.py
@@ -34,7 +34,8 @@
 PIECE = 16
 ORDER = (0, 1, 2, 3, 4, 5, 6, 7)
 WAITING = (1, 1, 1, 1, 1, 1, 1, 1)
-READY = (0.0, 5.8, 9.6, 13.5)
+READY = (0.0, 3.9, 11.6, 15.4)
+SUMS = 6.0
 LATENCY = 3.9
 EARLY = ((8, 7),)
 TAIL = 0
@@ -138,8 +139,7 @@
     load_sem,
     kv_sem,
     halo_sem,
-    ids_send,
-    ids_recv,
+    ids_sem,
     rs_send,
     rs_recv,
     d_send,
@@ -222,7 +222,7 @@
         for i, src in enumerate((kt_hbm, vt_hbm)):
             kv_loads.append(
                 pltpu.make_async_copy(
-                    src.at[:, cols], kv.at[b + 1, pl.ds(i * HD, HD)], kv_sem.at[2 * b + i]
+                    src.at[:, cols], kv.at[b + 1, pl.ds(i * HD, HD)], kv_sem.at[0]
                 )
             )
     barrier = pltpu.get_barrier_semaphore()
@@ -318,7 +318,7 @@
             src_ref=src.at[half, rows],
             dst_ref=dst.at[half, rows],
             send_sem=rs_send.at[group],
-            recv_sem=rs_recv.at[kind * QUARTERS + q],
+            recv_sem=rs_recv.at[min(kind, 2) * QUARTERS + q],
             device_id=device,
             device_id_type=MESH,
         )
@@ -346,13 +346,14 @@
         return pltpu.make_async_remote_copy(
             src_ref=ids_ref.at[0],
             dst_ref=ids_ref.at[m],
-            send_sem=ids_send.at[m],
-            recv_sem=ids_recv.at[m],
+            send_sem=ids_sem.at[0],
+            recv_sem=ids_sem.at[1],
             device_id=to_x(-m),
             device_id_type=MESH,
         )
 
-    for copy in kv_loads + small:
+    pltpu.make_async_copy(kv.at[pl.ds(1, TP)], kv.at[pl.ds(1, TP)], kv_sem.at[0]).wait()
+    for copy in small:
         copy.wait()
     attend(1, 1)
     pl.semaphore_wait(barrier, len(greeted))
@@ -369,8 +370,16 @@
     place[2] = placing(position_c)
     halo.wait_recv()
     attend(0, 0)
-    for m in range(1, TP):
-        ids_copy(m).wait_recv()
+    others = ids_ref.at[pl.ds(1, TP - 1)]
+    ids_all = pltpu.make_async_remote_copy(
+        src_ref=others,
+        dst_ref=others,
+        send_sem=ids_sem.at[0],
+        recv_sem=ids_sem.at[1],
+        device_id=right,
+        device_id_type=MESH,
+    )
+    ids_all.wait_recv()
 
     def arrange(m, placed):
         att_c[m] = mm(placed, att[lax.rem(x + m, TP)]).astype(BF)
@@ -387,12 +396,10 @@
     sm[0] = project(prior, 0).astype(BF)
     alone(0)
     first_leg(1)
-    first_leg(2)
     cbuf[0, :, pl.ds(0, HALF)] = project(after, 0)
     cbuf[1, :, pl.ds(0, HALF)] = project(prior, 1)
     joined(0)
     alone(1)
-    first_leg(3)
     large[0].wait()
     large[1].wait()
     arrange(0, place[2])
@@ -400,6 +407,8 @@
         cols = pl.ds(half * HALF, HALF)
         acc[:, cols] = project(0, half) + mm(place[2], res_ref[:, cols])
     joined(1)
+    first_leg(2)
+    first_leg(3)
     alone(2)
 
     t_lane = iota((E, T), 1)
@@ -437,13 +446,17 @@
             n = prefix(way, hop)
             if n < T:
                 ring[hop - 1, way, pl.ds(n, T - n)] = jnp.zeros((T - n, D), BF)
-    joined(2)
-    alone(3)
 
     def prepare(q):
-        for kind in range(2, 6):
-            rs_copy(kind, q).wait_recv()
         rows = pl.ds(q * CH, CH)
+        pltpu.make_async_remote_copy(
+            src_ref=acc.at[rows],
+            dst_ref=acc.at[rows],
+            send_sem=rs_send.at[0],
+            recv_sem=rs_recv.at[2 * QUARTERS + q],
+            device_id=right,
+            device_id_type=MESH,
+        ).wait_recv()
         square = jnp.zeros((CH, 1), F32)
         for half in range(2):
             cols = pl.ds(half * HALF, HALF)
@@ -484,7 +497,7 @@
         return pltpu.make_async_remote_copy(
             src_ref=src,
             dst_ref=ring.at[hop - 1, way, rows],
-            send_sem=d_send.at[hop_index(way, hop)],
+            send_sem=d_send.at[hop - 1],
             recv_sem=d_recv.at[index],
             device_id=ahead[way],
             device_id_type=MESH,
@@ -496,7 +509,7 @@
         return pltpu.make_async_remote_copy(
             src_ref=src,
             dst_ref=meta.at[hop - 1, way],
-            send_sem=m_send.at[index],
+            send_sem=m_send.at[way],
             recv_sem=m_recv.at[index],
             device_id=ahead[way],
             device_id_type=MESH,
@@ -507,7 +520,6 @@
     prepare(0)
     for way in range(2):
         packet_copy(way, 1, 0).start()
-    joined(QUARTERS - 1)
 
     def hop_table(hop):
         picked_t = jnp.zeros((1, T), F32)
@@ -524,7 +536,7 @@
         return pltpu.make_async_remote_copy(
             src_ref=buffer_from.at[hop - 1, peer_rank(k)],
             dst_ref=buffer_to.at[hop - 1, me],
-            send_sem=sends.at[hop - 1],
+            send_sem=sends.at[0],
             recv_sem=recvs.at[hop - 1],
             device_id=peer(k),
             device_id_type=MESH,
@@ -535,7 +547,7 @@
         return pltpu.make_async_remote_copy(
             src_ref=buffer_from.at[hop - 1, blocks],
             dst_ref=buffer_to.at[hop - 1, blocks],
-            send_sem=sends.at[hop - 1],
+            send_sem=sends.at[0],
             recv_sem=recvs.at[hop - 1],
             device_id=peer(1),
             device_id_type=MESH,
@@ -581,7 +593,7 @@
         return pltpu.make_async_remote_copy(
             src_ref=ret.at[hop, way, rows],
             dst_ref=ret.at[hop - 1, way, rows],
-            send_sem=b_send.at[hop_index(way, hop)],
+            send_sem=b_send.at[hop - 1],
             recv_sem=b_recv.at[index],
             device_id=behind[way],
             device_id_type=MESH,
@@ -635,12 +647,18 @@
     ready = list(READY) + [READY[-1]] * (T // PIECE - QUARTERS)
     events = ring_order(prefix, ORDER, ready, WAITING, LATENCY)
     prepared = 1
+    sums_left = True
     missing = {
         hop: sum(prefix(way, hop) // PIECE for way in range(2)) for hop in range(1, LAST + 1)
     }
     later = []
     seen = set()
     for when, action, way, piece, hop in events:
+        if sums_left and when >= SUMS:
+            joined(2)
+            alone(3)
+            joined(3)
+            sums_left = False
         while later and later[0][0] <= when:
             experts(*later.pop(0)[1])
         if action == "own":
@@ -656,7 +674,11 @@
         pass_on(way, hop, piece)
         missing[hop] -= 1
         if missing[hop] == 0:
+            if hop == LAST - 3 and missing[LAST - 2]:
+                continue
             select(hop)
+            if hop == LAST - 2 and not missing[LAST - 3]:
+                select(LAST - 3)
             for group in EARLY:
                 if hop in group and not any(missing[h] for h in group):
                     later.append((when + 12.0, group))
@@ -710,8 +732,7 @@
         out_ref[:, cols] = (mm_tn(place[2], stream[:, cols]) + mm_tn(unsort, came)).astype(BF)
 
     halo.wait_send()
-    for m in range(1, TP):
-        ids_copy(m).wait_send()
+    ids_all.wait_send()
     for group, (src, dst) in enumerate(((s2, r2), (sp, rp), (sm, rm))):
         pltpu.make_async_remote_copy(
             src_ref=src,
@@ -721,22 +742,24 @@
             device_id=right,
             device_id_type=MESH,
         ).wait_send()
+    def all_left(ref, sem):
+        pltpu.make_async_remote_copy(
+            src_ref=ref,
+            dst_ref=ref,
+            send_sem=sem,
+            recv_sem=halo_sem.at[1],
+            device_id=right,
+            device_id_type=MESH,
+        ).wait_send()
+
+    for hop in range(1, LAST + 1):
+        count = prefix(0, hop) + prefix(1, hop)
+        all_left(acc.at[pl.ds(0, count // 2)], d_send.at[hop - 1])
+        all_left(acc.at[pl.ds(0, count // 2)], b_send.at[hop - 1])
     for way in range(2):
-        for hop in range(1, HOPS[way] + 1):
-            meta_copy(way, hop).wait_send()
-            rows = pl.ds(0, prefix(way, hop))
-            for buffer, sems, recvs in ((ring, d_send, d_recv), (ret, b_send, b_recv)):
-                pltpu.make_async_remote_copy(
-                    src_ref=buffer.at[hop - 1, way, rows],
-                    dst_ref=buffer.at[hop - 1, way, rows],
-                    send_sem=sems.at[hop_index(way, hop)],
-                    recv_sem=recvs.at[0],
-                    device_id=ahead[way],
-                    device_id_type=MESH,
-                ).wait_send()
-    for hop in range(1, LAST + 1):
-        plane_all(sel, xin, p_send, p_recv, hop).wait_send()
-        plane_all(yout, zin, y_send, y_recv, hop).wait_send()
+        all_left(meta.at[pl.ds(0, HOPS[way]), way], m_send.at[way])
+    all_left(xin.at[:, pl.ds(0, PL - 1)], p_send.at[0])
+    all_left(zin.at[:, pl.ds(0, PL - 1)], y_send.at[0])
 
 
 def solution(mesh):
@@ -818,21 +841,20 @@
                 vm((HOP + 1, 2, T, D), BF),
                 vm((2, T, D), F32),
                 dma((10,)),
-                dma((2 * tp_count,)),
+                dma((1,)),
                 dma((2,)),
-                dma((tp_count,)),
-                dma((tp_count,)),
+                dma((2,)),
                 dma((3,)),
-                dma((6 * quarters,)),
-                dma((2 * HOP,)),
+                dma((3 * quarters,)),
+                dma((HOP,)),
                 dma((pieces,)),
-                dma((2 * HOP,)),
-                dma((2 * HOP,)),
+                dma((2,)),
+                dma((2 * HOP - 1,)),
+                dma((1,)),
+                dma((HOP,)),
+                dma((1,)),
                 dma((HOP,)),
                 dma((HOP,)),
-                dma((HOP,)),
-                dma((HOP,)),
-                dma((2 * HOP,)),
                 dma((pieces,)),
             ],
             compiler_params=pltpu.CompilerParams(

time: 197 us -> 197 us (level)
  no operation moved by 1% of the time
where the time goes in v7:
time: 197 us; the launch traced here: 196 us
  Pallas kernels  195 us (99%)
    pallas_call x1, Pallas kernels, on_device(): pl.pallas_call(functools.partial(layer, dims), out_shape=jax.ShapeDtypeSt...  195 us

profile of v7, /device:TPU:33, one launch (start us, length us, event | category | flops | bytes accessed | tf_op | source)
XLA Modules:
  0.0 196.4 jit_solution(2619020157568099854)
XLA Ops:
  0.0 194.6 %shard_map.118 = bf16[128,2048]{1,0:T(8,128)(2,1)} custom-call(bf16[512,512]{1,0:T(8,128)(2,1)} %q_hbm.1, bf16[64,512]{1,0:T(8,128)(2,1)} %bitcast.10, bf16[64,512]{1,0:T(8,128)(2,1)} %bitcast.11, f32[1,8]{1,0:T(1,128)} %bitcast.15, bf16[512,2048]{1,0:T(8,128)(2,1)} %wo_hbm.1, bf16[128,2048]{1,0:T(8,128)(2,1)} %res_hbm.1, f32[1,2048]{1,0:T(1,128)} %bitcast.12, ...), custom_call_target="tpu_custom_call" | custom-call | tf_op jit(solution)/shard_map/pallas_call | solution.py:803
  194.6 1.9 copy.14

commit v8 on v7

--- a/solution.py
+++ b/solution.py
@@ -36,10 +36,7 @@
 WAITING = (1, 1, 1, 1, 1, 1, 1, 1)
 READY = (0.0, 3.9, 11.6, 15.4)
 SUMS = 6.0
-LATENCY = 3.9
-EARLY = ((8, 7),)
-TAIL = 0
-PEERS = (1, 2, 3, 4, 5, 6, 7)
+LATENCY = 3.0
 
 
 def prefix_rows(hops, rows, share):
@@ -101,7 +98,7 @@
     wg_hbm,
     wu_hbm,
     wd_hbm,
-    out_ref,
+    out_hbm,
     qv,
     kv,
     wo,
@@ -136,6 +133,7 @@
     zin,
     ret,
     cbuf,
+    outv,
     load_sem,
     kv_sem,
     halo_sem,
@@ -563,7 +561,7 @@
             cols = pl.ds(n * COLS, COLS)
             rows = ring[hop - 1, :, :, cols].reshape(2 * T, COLS)
             sel[hop - 1, :, :, cols] = mm_tn(hot, rows).reshape(PL, GR, COLS).astype(BF)
-        for k in PEERS:
+        for k in range(1, PL):
             plane_copy(sel, xin, p_send, p_recv, hop, k).start()
         xin[hop - 1, me] = sel[hop - 1, me]
 
@@ -583,7 +581,7 @@
                 part = product[i * SEL : (i + 1) * SEL]
                 yout[hop - 1, :, :, cols] = part.reshape(PL, GR, COLS).astype(BF)
         for hop in hops:
-            for k in PEERS:
+            for k in range(1, PL):
                 plane_copy(yout, zin, y_send, y_recv, hop, k).start()
             zin[hop - 1, me] = yout[hop - 1, me]
 
@@ -679,45 +677,19 @@
             select(hop)
             if hop == LAST - 2 and not missing[LAST - 3]:
                 select(LAST - 3)
-            for group in EARLY:
+            for group in ((LAST, LAST - 1),):
                 if hop in group and not any(missing[h] for h in group):
                     later.append((when + 12.0, group))
     for _, group in later:
         experts(*group)
-    if TAIL == 0:
-        send_back(8)
-        send_back(7)
-        experts(6, 5)
-        experts(1, 2)
-        experts(3, 4)
-        rest = range(6, 0, -1)
-    elif TAIL == 1:
-        send_back(8)
-        send_back(7)
-        experts(6)
-        experts(5)
-        send_back(6)
-        experts(1, 2)
-        experts(3, 4)
-        rest = range(5, 0, -1)
-    elif TAIL == 2:
-        send_back(8)
-        experts(5)
-        send_back(7)
-        experts(6)
-        experts(3, 4)
-        send_back(6)
-        experts(1, 2)
-        rest = range(5, 0, -1)
-    elif TAIL == 3:
-        send_back(8)
-        send_back(7)
-        experts(5)
-        send_back(6)
-        experts(1, 2)
-        experts(3, 4)
-        rest = range(5, 0, -1)
-    for hop in rest:
+    send_back(LAST)
+    send_back(LAST - 1)
+    experts(LAST - 2)
+    experts(LAST - 3)
+    send_back(LAST - 2)
+    experts(1, 2)
+    experts(3, 4)
+    for hop in range(LAST - 3, 0, -1):
         send_back(hop)
 
     for j in range(T // PIECE):
@@ -725,11 +697,16 @@
         for way in range(2):
             back_copy(way, 1, j).wait_recv()
         ret[0, 1, rows] = (ret[0, 1, rows].astype(F32) + acc[rows]).astype(BF)
+    stores = []
     unsort = place[pl.ds(0, 2)].reshape(2 * T, T)
     for n in range(D // COLS):
         cols = pl.ds(n * COLS, COLS)
         came = ret[0, :, :, cols].reshape(2 * T, COLS)
-        out_ref[:, cols] = (mm_tn(place[2], stream[:, cols]) + mm_tn(unsort, came)).astype(BF)
+        outv[:, cols] = (mm_tn(place[2], stream[:, cols]) + mm_tn(unsort, came)).astype(BF)
+        stores.append(
+            pltpu.make_async_copy(outv.at[:, cols], out_hbm.at[:, cols], load_sem.at[n])
+        )
+        stores[-1].start()
 
     halo.wait_send()
     ids_all.wait_send()
@@ -760,6 +737,8 @@
         all_left(meta.at[pl.ds(0, HOPS[way]), way], m_send.at[way])
     all_left(xin.at[:, pl.ds(0, PL - 1)], p_send.at[0])
     all_left(zin.at[:, pl.ds(0, PL - 1)], y_send.at[0])
+    for copy in stores:
+        copy.wait()
 
 
 def solution(mesh):
@@ -795,7 +774,6 @@
         dma = pltpu.SemaphoreType.DMA
         vm = pltpu.VMEM
         any_space = pl.BlockSpec(memory_space=pl.ANY)
-        in_vmem = pl.BlockSpec(memory_space=pltpu.VMEM)
         dims = (T, D, Z, tp_count, sp_count, CAP, HEADS, HD)
         quarters = T // (PL * CAP)
         prefix = prefix_rows((HOP, HOP - 1), T, PL * CAP)
@@ -804,7 +782,7 @@
             functools.partial(layer, dims),
             out_shape=jax.ShapeDtypeStruct((T, D), BF),
             in_specs=[any_space] * 12,
-            out_specs=in_vmem,
+            out_specs=any_space,
             scratch_shapes=[
                 vm(queries.shape, BF),
                 vm((tp_count + 1, 2 * HD, T), BF),
@@ -840,6 +818,7 @@
                 vm((HOP, PL, GR, D), BF),
                 vm((HOP + 1, 2, T, D), BF),
                 vm((2, T, D), F32),
+                vm((T, D), BF),
                 dma((10,)),
                 dma((1,)),
                 dma((2,)),

time: 197 us -> 194 us (0.985)
  Pallas kernels: 195 us -> 192 us
    pallas_call x1, Pallas kernels: 195 us -> 192 us  [on_device(): pl.pallas_call(functools.partial(layer, dims), out_shape=jax.ShapeDtypeSt...]
where the time goes in v8:
time: 194 us
  Pallas kernels  192 us (99%)
    pallas_call x1, Pallas kernels, on_device(): pl.pallas_call(functools.partial(layer, dims), out_shape=jax.ShapeDtypeSt...  192 us

profile of v8, /device:TPU:33, one launch (start us, length us, event | category | flops | bytes accessed | tf_op | source)
XLA Modules:
  0.0 194.3 jit_solution(9517876809702069499)
XLA Ops:
  0.0 192.4 %shard_map.118 = bf16[128,2048]{1,0:T(8,128)(2,1)} custom-call(bf16[512,512]{1,0:T(8,128)(2,1)} %q_hbm.1, bf16[64,512]{1,0:T(8,128)(2,1)} %bitcast.10, bf16[64,512]{1,0:T(8,128)(2,1)} %bitcast.11, f32[1,8]{1,0:T(1,128)} %bitcast.15, bf16[512,2048]{1,0:T(8,128)(2,1)} %wo_hbm.1, bf16[128,2048]{1,0:T(8,128)(2,1)} %res_hbm.1, f32[1,2048]{1,0:T(1,128)} %bitcast.12, ...), custom_call_target="tpu_custom_call" | custom-call | tf_op jit(solution)/shard_map/pallas_call | solution.py:781
  192.4 1.9 copy.14

commit v9 on v8

--- a/solution.py
+++ b/solution.py
@@ -552,16 +552,16 @@
         )
 
     COLS = 512
+    far_first = sorted(range(1, PL), key=lambda k: -min(k % TP, TP - k % TP))
 
     def select(hop):
-        hop_table(hop)
         spot = (iota((2 * T, SEL), 0) + 1).astype(F32)
         hot = jnp.where(spot == table[hop - 1, 0:1, 0:SEL], 1.0, 0.0).astype(BF)
         for n in range(D // COLS):
             cols = pl.ds(n * COLS, COLS)
             rows = ring[hop - 1, :, :, cols].reshape(2 * T, COLS)
             sel[hop - 1, :, :, cols] = mm_tn(hot, rows).reshape(PL, GR, COLS).astype(BF)
-        for k in range(1, PL):
+        for k in far_first:
             plane_copy(sel, xin, p_send, p_recv, hop, k).start()
         xin[hop - 1, me] = sel[hop - 1, me]
 
@@ -581,7 +581,7 @@
                 part = product[i * SEL : (i + 1) * SEL]
                 yout[hop - 1, :, :, cols] = part.reshape(PL, GR, COLS).astype(BF)
         for hop in hops:
-            for k in range(1, PL):
+            for k in far_first:
                 plane_copy(yout, zin, y_send, y_recv, hop, k).start()
             zin[hop - 1, me] = yout[hop - 1, me]
 
@@ -669,6 +669,8 @@
         if (way, hop) not in seen:
             seen.add((way, hop))
             meta_on(way, hop)
+            if all((w, hop) in seen for w in range(2) if hop <= HOPS[w]):
+                hop_table(hop)
         pass_on(way, hop, piece)
         missing[hop] -= 1
         if missing[hop] == 0:
@@ -679,7 +681,7 @@
                 select(LAST - 3)
             for group in ((LAST, LAST - 1),):
                 if hop in group and not any(missing[h] for h in group):
-                    later.append((when + 12.0, group))
+                    later.append((when + 10.0, group))
     for _, group in later:
         experts(*group)
     send_back(LAST)

time: 194 us -> 194 us (level)
  no operation moved by 1% of the time
where the time goes in v9:
time: 194 us
  Pallas kernels  192 us (99%)
    pallas_call x1, Pallas kernels, on_device(): pl.pallas_call(functools.partial(layer, dims), out_shape=jax.ShapeDtypeSt...  192 us

profile of v9, /device:TPU:33, one launch (start us, length us, event | category | flops | bytes accessed | tf_op | source)
XLA Modules:
  0.0 193.7 jit_solution(12565980997210268800)
XLA Ops:
  0.0 191.8 %shard_map.118 = bf16[128,2048]{1,0:T(8,128)(2,1)} custom-call(bf16[512,512]{1,0:T(8,128)(2,1)} %q_hbm.1, bf16[64,512]{1,0:T(8,128)(2,1)} %bitcast.10, bf16[64,512]{1,0:T(8,128)(2,1)} %bitcast.11, f32[1,8]{1,0:T(1,128)} %bitcast.15, bf16[512,2048]{1,0:T(8,128)(2,1)} %wo_hbm.1, bf16[128,2048]{1,0:T(8,128)(2,1)} %res_hbm.1, f32[1,2048]{1,0:T(1,128)} %bitcast.12, ...), custom_call_target="tpu_custom_call" | custom-call | tf_op jit(solution)/shard_map/pallas_call | solution.py:783
  191.8 1.9 copy.14
